TPU v7x, 32 devices: a whole 2x2x4 slice. The times are simulated.
32 devices in a mesh: kv: 8 (over z, x), tp: 4 (over y, core).
Axes of the slice: x: 2, y: 2, z: 4, core: 2. Of those that a mesh axis runs over, the one named last changes fastest.
Arguments:
- tokens: bfloat16 [256, 2048], P('kv', 'tp'), may hold values from -60 to 60, as said below
- memory: float32 [256, 8, 128, 128], P('kv', 'tp'), may hold values from -0.6 to 0.6
- normalizer: float32 [256, 8, 128], P('kv', 'tp'), may hold values from -0.6 to 0.6
- stabilizer: float32 [256, 8], P('kv', 'tp'), may hold values from -4 to 4
- norm_gain: float32 [2048], replicated, may hold values from 0.1 to 1.9
- query_weight: bfloat16 [2048, 1024], P(None, 'tp'), may hold values from -0.125 to 0.125
- key_weight: bfloat16 [2048, 1024], P(None, 'tp'), may hold values from -0.125 to 0.125
- value_weight: bfloat16 [2048, 1024], P(None, 'tp'), may hold values from -0.125 to 0.125
- outgate_weight: bfloat16 [2048, 1024], P(None, 'tp'), may hold values from -0.125 to 0.125
- input_gate_weight: bfloat16 [2048, 8], replicated, may hold values from -0.125 to 0.125
- forget_gate_weight: bfloat16 [2048, 8], replicated, may hold values from -0.125 to 0.125
- forget_bias: float32 [8], replicated, may hold values from -1 to 5
- memory_gain: float32 [1024], P('tp'), may hold values from 0.1 to 1.9
- proj_weight: bfloat16 [1024, 2048], P(None, 'tp'), may hold values from -0.1875 to 0.1875
- ffn_gain: float32 [2048], P('tp'), may hold values from 0.1 to 1.9
- up_weight: bfloat16 [2048, 8192], P('tp', 'kv'), may hold values from -0.125 to 0.125
- down_weight: bfloat16 [8192, 2048], P('kv', 'tp'), may hold values from -0.0625 to 0.0625
Outputs:
- layer_out: bfloat16 [256, 2048], P('kv', 'tp')
- memory_new: float32 [256, 8, 128, 128], P('kv', 'tp')
- normalizer_new: float32 [256, 8, 128], P('kv', 'tp')
- stabilizer_new: float32 [256, 8], P('kv', 'tp')
Inputs may be any that keep to these rules, and one draw needn't show every extreme that they name: `tokens`: activations whose feature blocks and rows differ in scale.
All inputs are finite; a program needn't handle non-finite values.
Results may differ from a plain program's by a relative error of at most 0.0095.
Values may be sent and summed in bfloat16 or wider, within the bound.
No kernel may reach another device: no remote copies, remote signals or barrier semaphores. Data moves between devices by JAX's collectives and lax.ppermute only.
A program may use at most 64 MiB of HBM per device.

v0:
```python
import jax
import jax.numpy as jnp
from jax import lax
from jax.sharding import PartitionSpec as P

D = 2048
DK = 128
DV = 128


EPS = 1e-06


def per_device(
    tokens,
    memory,
    normalizer,
    stabilizer,
    norm_gain,
    query_weight,
    key_weight,
    value_weight,
    outgate_weight,
    input_gate_weight,
    forget_gate_weight,
    forget_bias,
    memory_gain,
    proj_weight,
    ffn_gain,
    up_weight,
    down_weight,
):
    own_rows = tokens.shape[0]
    heads_here = memory.shape[1]
    first_head = lax.axis_index("tp") * heads_here
    full_rows = lax.all_gather(tokens, "tp", axis=1, tiled=True)
    rows_f = full_rows.astype(jnp.float32)
    scale_one = lax.rsqrt(jnp.mean(rows_f * rows_f, axis=-1, keepdims=True) + EPS)
    normed = (rows_f * scale_one * norm_gain).astype(jnp.bfloat16)
    query = jnp.dot(normed, query_weight, preferred_element_type=jnp.float32).astype(jnp.bfloat16)
    keys = jnp.dot(normed, key_weight, preferred_element_type=jnp.float32).astype(jnp.bfloat16)
    values = jnp.dot(normed, value_weight, preferred_element_type=jnp.float32).astype(jnp.bfloat16)
    gate_out = jnp.dot(normed, outgate_weight, preferred_element_type=jnp.float32).astype(
        jnp.bfloat16
    )
    input_cols = lax.dynamic_slice_in_dim(input_gate_weight, first_head, heads_here, 1)
    forget_cols = lax.dynamic_slice_in_dim(forget_gate_weight, first_head, heads_here, 1)
    bias_here = lax.dynamic_slice_in_dim(forget_bias, first_head, heads_here, 0)
    input_log = jnp.dot(normed, input_cols, preferred_element_type=jnp.float32)
    forget_log = jax.nn.log_sigmoid(
        jnp.dot(normed, forget_cols, preferred_element_type=jnp.float32) + bias_here
    )
    query_f = query.astype(jnp.float32).reshape(own_rows, heads_here, DK)
    keys_f = keys.astype(jnp.float32).reshape(own_rows, heads_here, DK) * DK ** (-0.5)
    values_f = values.astype(jnp.float32).reshape(own_rows, heads_here, DV)
    stab_new = jnp.maximum(forget_log + stabilizer, input_log)
    keep = jnp.exp(forget_log + stabilizer - stab_new)
    admit = jnp.exp(input_log - stab_new)
    memory_new = (
        keep[..., None, None] * memory
        + admit[..., None, None] * values_f[..., :, None] * keys_f[..., None, :]
    )
    normalizer_new = keep[..., None] * normalizer + admit[..., None] * keys_f
    numer = jnp.einsum("bhed,bhd->bhe", memory_new, query_f, precision=lax.Precision.HIGHEST)
    denom = jnp.sum(normalizer_new * query_f, axis=-1)
    cell = numer / jnp.maximum(jnp.abs(denom), 1.0)[..., None]
    mixed = (
        cell.reshape(own_rows, heads_here * DV)
        * memory_gain
        * jax.nn.sigmoid(gate_out.astype(jnp.float32))
    ).astype(jnp.bfloat16)
    projected = jnp.dot(
        lax.all_gather(mixed, "tp", axis=1, tiled=True),
        proj_weight,
        preferred_element_type=jnp.float32,
    )
    second = (tokens.astype(jnp.float32) + projected).astype(jnp.bfloat16)
    all_rows = lax.all_gather(second, "kv", axis=0, tiled=True)
    all_f = all_rows.astype(jnp.float32)
    square_sum = jnp.sum(all_f * all_f, axis=-1)
    scaled = (all_f * ffn_gain).astype(jnp.bfloat16)
    preact = jnp.dot(scaled, up_weight, preferred_element_type=jnp.float32)
    share = lax.psum_scatter(preact, "tp", scatter_dimension=1, tiled=True)
    square_sum = lax.psum(square_sum, "tp")
    scale_two = lax.rsqrt(square_sum / D + EPS)
    partial_hidden = jnp.square(jax.nn.relu(share * scale_two[:, None])).astype(jnp.bfloat16)
    hidden = lax.all_gather(partial_hidden, "tp", axis=1, tiled=True)
    summed = lax.psum_scatter(
        jnp.dot(hidden, down_weight, preferred_element_type=jnp.float32),
        "kv",
        scatter_dimension=0,
        tiled=True,
    )
    layer_out = (second.astype(jnp.float32) + summed).astype(jnp.bfloat16)
    return (layer_out, memory_new, normalizer_new, stab_new)


def solution(mesh):
    placed = (
        P("kv", "tp"),
        P("kv", "tp", None, None),
        P("kv", "tp", None),
        P("kv", "tp"),
        P(),
        P(None, "tp"),
        P(None, "tp"),
        P(None, "tp"),
        P(None, "tp"),
        P(),
        P(),
        P(),
        P("tp"),
        P(None, "tp"),
        P("tp"),
        P("tp", "kv"),
        P("kv", "tp"),
    )
    return jax.shard_map(
        per_device,
        mesh=mesh,
        in_specs=placed,
        out_specs=(P("kv", "tp"), P("kv", "tp", None, None), P("kv", "tp", None), P("kv", "tp")),
        check_vma=False,
    )
```

profile of v0, /device:TPU:0, one launch (start us, length us, event | category | flops | bytes accessed | tf_op | source)
XLA Modules:
  0.0 177.4 jit_solution(6909236550511588399)
XLA Ops:
  7.2 0.0 copy-start
  7.2 0.0 copy-start.7
  7.2 0.0 reduce-scatter.3.cloned.1.call-start
  7.2 6.9 %all_gather.12 = bf16[32,2048]{1,0:T(8,128)(2,1)S(1)} all-gather(bf16[32,512]{1,0:T(8,128)(2,1)} %param.17), channel_id=1, replica_groups=mesh['kv'=8,'tp'=4] {'tp'}, dimensions={1}, use_global_device_ids=true | all-gather | bytes 163840 | tf_op jit(solution)/shard_map/all_gather | solution.py:36
  14.1 0.1 fusion.13
  14.3 1.6 convolution_convert_fusion.1
  15.9 0.7 dynamic_slice.10
  16.6 1.0 fusion.23
  17.6 1.0 broadcast_multiply_fusion.2
  18.6 0.0 copy-start.9
  18.6 0.1 copy.21
  18.7 0.1 copy.24
  18.8 0.1 copy.22
  18.9 1.6 fusion.9
  20.5 1.6 fusion.8
  22.1 0.0 copy-done.7
  22.1 0.8 multiply_reduce_fusion
  22.9 3.7 %multiply_add_fusion = f32[32,2,128,128]{3,2,1,0:T(8,128)S(1)} fusion(f32[32,2,128,128]{3,2,1,0:T(8,128)} %param.18, f32[32,2,128]{2,1,0:T(2,128)S(1)} %get-tuple-element.9, f32[32,2,128]{2,1,0:T(2,128)S(1)} %get-tuple-element.10, f32[32,2]{1,0:T(8,128)S(1)} %copy.21), kind=kLoop, calls=%fused_computation | loop fusion | flops 3145728 | bytes 8454400 | tf_op jit(solution)/shard_map/add | solution.py:60
  26.6 0.0 copy-done.9
  26.6 0.0 copy-start.1
  26.6 2.0 %copy-done.1 = f32[32,2,128,128]{3,2,1,0:T(8,128)} copy-done((f32[32,2,128,128]{3,2,1,0:T(8,128)}, f32[32,2,128,128]{3,2,1,0:T(8,128)S(1)}, u32[]{:S(2)}) %copy-start.1) | copy-done | bytes 4194328
  28.6 0.0 copy-start.3
  28.6 0.0 copy-start.5
  28.6 0.0 copy-start.10
  28.6 0.0 copy-start.2
  28.6 0.0 copy-start.6
  28.6 0.0 copy-start.8
  28.6 3.3 %fusion.34 = f32[32,2,1,128]{3,2,1,0:T(1,128)S(1)} fusion(f32[32,2,128,128]{3,2,1,0:T(8,128)S(1)} %multiply_add_fusion, bf16[32,2,128,1]{2,3,1,0:T(2,128)(2,1)S(1)} %reshape.70), kind=kOutput, calls=%fused_computation.51 | convolution fusion | flops 12582912 | bytes 4243456 | tf_op jit(solution)/shard_map/bhed,bhd->bhe/dot_general | solution.py:64
  32.0 0.0 copy-start.4
  32.0 0.1 broadcast_divide_fusion
  32.1 0.0 copy-done.3
  32.1 0.0 copy-done.5
  32.1 0.0 copy-done.10
  32.2 0.3 fusion.7
  32.5 5.4 %all_gather.13 = bf16[32,1024]{1,0:T(8,128)(2,1)S(1)} all-gather(bf16[32,256]{1,0:T(8,128)(2,1)S(1)} %fusion.7), channel_id=1, replica_groups=mesh['kv'=8,'tp'=4] {'tp'}, dimensions={1}, use_global_device_ids=true | all-gather | bytes 81920 | tf_op jit(solution)/shard_map/all_gather | solution.py:73
  37.9 0.0 copy-done.2
  37.9 0.0 copy-done.6
  37.9 0.3 fusion
  38.2 31.4 %all_gather.14 = bf16[256,512]{1,0:T(8,128)(2,1)S(1)} all-gather(bf16[32,512]{1,0:T(8,128)(2,1)S(1)} %fusion), channel_id=1, replica_groups=mesh['kv'=8,'tp'=4] {'kv'}, dimensions={0}, use_global_device_ids=true | all-gather | bytes 294912 | tf_op jit(solution)/shard_map/all_gather | solution.py:78
  69.6 0.0 copy-done
  69.6 0.0 copy-done.8
  69.6 1.4 fusion.16
  71.0 0.0 reduce-scatter.3.cloned.1.call-update
  71.0 0.0 reduce-scatter.5.cloned.1.call-start
  71.1 0.1 fusion.12
  71.2 5.7 %psum.7 = f32[256]{0:T(256)S(1)} all-reduce(f32[256]{0:T(256)S(1)} %fusion.12), channel_id=1, replica_groups=mesh['kv'=8,'tp'=4] {'tp'}, use_global_device_ids=true, to_apply=%region_4.5 | all-reduce | flops 256 | bytes 2048 | tf_op jit(solution)/shard_map/psum | solution.py:84
  76.9 19.9 %reduce-scatter.3.cloned.1.call-done = f32[256,256]{1,0:T(8,128)} async-done(((f32[256,1024]{1,0:T(8,128)}), f32[256,256]{1,0:T(8,128)}) %reduce-scatter.3.cloned.1.call-update) | async-done | bytes 262160 | tf_op jit(solution)/shard_map/reduce_scatter | solution.py:83
  96.8 1.1 multiply_convert_fusion
  97.8 6.6 %all_gather.15 = bf16[256,1024]{1,0:T(8,128)(2,1)S(1)} all-gather(bf16[256,256]{1,0:T(8,128)(2,1)S(1)} %multiply_convert_fusion), channel_id=1, replica_groups=mesh['kv'=8,'tp'=4] {'tp'}, dimensions={1}, use_global_device_ids=true | all-gather | bytes 655360 | tf_op jit(solution)/shard_map/all_gather | solution.py:87
  104.4 0.0 copy-done.4
  104.4 1.2 fusion.35
  105.7 0.0 reduce-scatter.5.cloned.1.call-update
  105.7 63.4 %reduce-scatter.5.cloned.1.call-done = f32[32,512]{1,0:T(8,128)} async-done(((f32[256,512]{1,0:T(8,128)}), f32[32,512]{1,0:T(8,128)}) %reduce-scatter.5.cloned.1.call-update) | async-done | bytes 65552 | tf_op jit(solution)/shard_map/reduce_scatter | solution.py:88
  169.1 1.5 add_convert_fusion
  (8 shorter events, 0.1 us)
Async XLA Ops:
  7.2 62.4 %copy-start = (bf16[512,1024]{1,0:T(8,128)(2,1)S(1)}, bf16[512,1024]{1,0:T(8,128)(2,1)}, u32[]{:S(2)}) copy-start(bf16[512,1024]{1,0:T(8,128)(2,1)} %param.32) | copy-start | bytes 3145732
  7.2 14.9 %copy-start.7 = (f32[32,2,128]{2,1,0:T(2,128)S(1)}, f32[32,2,128]{2,1,0:T(2,128)}, u32[]{:S(2)}) copy-start(f32[32,2,128]{2,1,0:T(2,128)} %param.19) | copy-start | bytes 98308
  7.2 89.6 %reduce-scatter.3.cloned.1.call-start = ((), (), s32[]{:S(2)}) async-start(), calls=%async_computation.2 | async-start | bytes 1310720 | tf_op jit(solution)/shard_map/reduce_scatter | solution.py:83
  18.6 8.0 %copy-start.9 = (f32[32,2]{0,1:T(2,128)}, f32[32,2]{0,1:T(2,128)S(1)}, u32[]{:S(2)}) copy-start(f32[32,2]{0,1:T(2,128)S(1)} %get-tuple-element.8) | copy-start | bytes 772
  26.6 2.0 %copy-start.1 = (f32[32,2,128,128]{3,2,1,0:T(8,128)}, f32[32,2,128,128]{3,2,1,0:T(8,128)S(1)}, u32[]{:S(2)}) copy-start(f32[32,2,128,128]{3,2,1,0:T(8,128)S(1)} %multiply_add_fusion) | copy-start | bytes 12582916
  28.6 3.5 %copy-start.3 = (bf16[2048,256]{1,0:T(8,128)(2,1)S(1)}, bf16[2048,256]{1,0:T(8,128)(2,1)}, u32[]{:S(2)}) copy-start(bf16[2048,256]{1,0:T(8,128)(2,1)} %param.25) | copy-start | bytes 3145732
  28.6 3.5 %copy-start.5 = (f32[2048]{0:T(1024)S(1)}, f32[2048]{0:T(1024)}, u32[]{:S(2)}) copy-start(f32[2048]{0:T(1024)} %param.21) | copy-start | bytes 24580
  28.6 3.5 %copy-start.10 = (f32[256]{0:T(256)S(1)}, f32[256]{0:T(256)}, u32[]{:S(2)}) copy-start(f32[256]{0:T(256)} %param.29) | copy-start | bytes 3076
  28.6 9.3 %copy-start.2 = (bf16[1024,512]{1,0:T(8,128)(2,1)S(1)}, bf16[1024,512]{1,0:T(8,128)(2,1)}, u32[]{:S(2)}) copy-start(bf16[1024,512]{1,0:T(8,128)(2,1)} %param.30) | copy-start | bytes 3145732
  28.6 9.3 %copy-start.6 = (bf16[32,512]{1,0:T(8,128)(2,1)S(1)}, bf16[32,512]{1,0:T(8,128)(2,1)}, u32[]{:S(2)}) copy-start(bf16[32,512]{1,0:T(8,128)(2,1)} %param.17) | copy-start | bytes 98308
  28.6 40.9 %copy-start.8 = (f32[512]{0:T(512)S(1)}, f32[512]{0:T(512)}, u32[]{:S(2)}) copy-start(f32[512]{0:T(512)} %param.31) | copy-start | bytes 6148
  32.0 72.4 %copy-start.4 = (bf16[1024,512]{1,0:T(8,128)(2,1)S(1)}, bf16[1024,512]{1,0:T(8,128)(2,1)}, u32[]{:S(2)}) copy-start(bf16[1024,512]{1,0:T(8,128)(2,1)} %param.33) | copy-start | bytes 3145732
  71.0 98.1 %reduce-scatter.5.cloned.1.call-start = ((), (), s32[]{:S(2)}) async-start(), calls=%async_computation.3 | async-start | bytes 589824 | tf_op jit(solution)/shard_map/reduce_scatter | solution.py:88
Sparse Core Ops, SparseCore 0:
  71.1 25.5 reduce-scatter.2
  105.8 63.2 reduce-scatter.4
where the time goes:
time: 178 us; the launch traced here: 177 us
  waiting for transfers between devices  83.3 us (47%)
  blocking collectives  55.9 us (31%)
  between operations  14.2 us (8%)
  matrix products  13.3 us (7%)
  other arithmetic  7.4 us (4%)
  local copies, waits for them, and re-layouts  3.12 us (2%)
    reduce_scatter x1, waiting for transfers between devices, per_device(): lax.psum_scatter(jnp.dot(hidden, down_weight, preferred_element_type=jnp....  63.4 us
    all_gather x1, blocking collectives, per_device(): all_rows = lax.all_gather(second, 'kv', axis=0, tiled=True)  31.4 us
    reduce_scatter x1, waiting for transfers between devices, per_device(): share = lax.psum_scatter(preact, 'tp', scatter_dimension=1, tiled=True)  19.9 us
    all_gather x1, blocking collectives, per_device(): full_rows = lax.all_gather(tokens, 'tp', axis=1, tiled=True)  6.88 us
    all_gather x1, blocking collectives, per_device(): hidden = lax.all_gather(partial_hidden, 'tp', axis=1, tiled=True)  6.61 us
    psum x1, blocking collectives, per_device(): square_sum = lax.psum(square_sum, 'tp')  5.67 us
    all_gather x1, blocking collectives, per_device(): lax.all_gather(mixed, 'tp', axis=1, tiled=True)  5.41 us
    add x1, other arithmetic, per_device(): keep[..., None, None] * memory  3.69 us
  transfers between devices with their start and end apart: 2, of which 2 were waited for; matrix products, arithmetic and copies ran while one was open for 0% of the time, Pallas kernels for 0%

commit v1 on v0

--- a/solution.py
+++ b/solution.py
@@ -9,6 +9,17 @@
 
 
 EPS = 1e-06
+
+
+def sum_over(partial, axis, dim):
+    parts = lax.axis_size(axis)
+    sent = partial.astype(jnp.bfloat16)
+    if dim == 1:
+        sent = sent.reshape(sent.shape[0], parts, -1).transpose(1, 0, 2)
+    else:
+        sent = sent.reshape(parts, -1, sent.shape[1])
+    got = lax.all_to_all(sent, axis, 0, 0, tiled=True)
+    return jnp.sum(got.astype(jnp.float32), axis=0)
 
 
 def per_device(
@@ -75,22 +86,20 @@
         preferred_element_type=jnp.float32,
     )
     second = (tokens.astype(jnp.float32) + projected).astype(jnp.bfloat16)
-    all_rows = lax.all_gather(second, "kv", axis=0, tiled=True)
+    groups = lax.axis_size("kv")
+    all_rows = lax.all_to_all(
+        jnp.broadcast_to(second, (groups,) + second.shape), "kv", 0, 0, tiled=True
+    ).reshape(groups * own_rows, second.shape[1])
     all_f = all_rows.astype(jnp.float32)
     square_sum = jnp.sum(all_f * all_f, axis=-1)
     scaled = (all_f * ffn_gain).astype(jnp.bfloat16)
     preact = jnp.dot(scaled, up_weight, preferred_element_type=jnp.float32)
-    share = lax.psum_scatter(preact, "tp", scatter_dimension=1, tiled=True)
+    share = sum_over(preact, "tp", 1)
     square_sum = lax.psum(square_sum, "tp")
     scale_two = lax.rsqrt(square_sum / D + EPS)
     partial_hidden = jnp.square(jax.nn.relu(share * scale_two[:, None])).astype(jnp.bfloat16)
     hidden = lax.all_gather(partial_hidden, "tp", axis=1, tiled=True)
-    summed = lax.psum_scatter(
-        jnp.dot(hidden, down_weight, preferred_element_type=jnp.float32),
-        "kv",
-        scatter_dimension=0,
-        tiled=True,
-    )
+    summed = sum_over(jnp.dot(hidden, down_weight, preferred_element_type=jnp.float32), "kv", 0)
     layer_out = (second.astype(jnp.float32) + summed).astype(jnp.bfloat16)
     return (layer_out, memory_new, normalizer_new, stab_new)
 

time: 178 us -> 82 us (0.46)
  waiting for transfers between devices: 83.3 us -> 0.01 us
  between operations: 14.2 us -> 0.91 us
  starting transfers between devices: 0.08 us -> 3.47 us
  blocking collectives: 55.9 us -> 57.7 us
  matrix products: 13.3 us -> 11.5 us
    reduce_scatter x2 -> x0, waiting for transfers between devices: 83.3 us -> none  [the longest x1 63.4 us: per_device(): lax.psum_scatter(jnp.dot(hidden, down_weight, preferred_element_type=jnp....]
    all_gather x1 -> x0, blocking collectives: 31.4 us -> none  [per_device(): all_rows = lax.all_gather(second, 'kv', axis=0, tiled=True)]
    all_to_all x0 -> x2, blocking collectives: none -> 28 us  [the longest x1 15.2 us: per_device(): lax.all_to_all(jnp.broadcast_to(second, (groups,) + second.shape), 'kv',...]
    psum x1, blocking collectives: 5.67 us -> 10 us  [per_device(): square_sum = lax.psum(square_sum, 'tp')]
    all_to_all x0 -> x1, starting transfers between devices: none -> 3.47 us  [sum_over(): got = lax.all_to_all(sent, axis, 0, 0, tiled=True)]
    unnamed x22, local copies, waits for them, and re-layouts: 2.06 us -> 0.07 us
  transfers between devices with their start and end apart: 2 -> 1, of which waited for: 2 -> 0; matrix products, arithmetic and copies ran while one was open for 0% -> 0% of each run, Pallas kernels for 0% -> 0%
where the time goes in v1:
time: 82 us; the launch traced here: 81.4 us
  blocking collectives  57.7 us (70%)
  matrix products  11.5 us (14%)
  other arithmetic  5.76 us (7%)
  starting transfers between devices  3.47 us (4%)
  local copies, waits for them, and re-layouts  2.06 us (3%)
  between operations  0.91 us (1%)
    all_to_all x1, blocking collectives, per_device(): lax.all_to_all(jnp.broadcast_to(second, (groups,) + second.shape), 'kv',...  15.2 us
    all_to_all x1, blocking collectives, sum_over(): got = lax.all_to_all(sent, axis, 0, 0, tiled=True)  12.8 us
    psum x1, blocking collectives, per_device(): square_sum = lax.psum(square_sum, 'tp')  10 us
    all_gather x1, blocking collectives, per_device(): hidden = lax.all_gather(partial_hidden, 'tp', axis=1, tiled=True)  7.32 us
    all_gather x1, blocking collectives, per_device(): full_rows = lax.all_gather(tokens, 'tp', axis=1, tiled=True)  6.88 us
    all_gather x1, blocking collectives, per_device(): lax.all_gather(mixed, 'tp', axis=1, tiled=True)  5.41 us
    add x1, other arithmetic, per_device(): keep[..., None, None] * memory  3.69 us
    all_to_all x1, starting transfers between devices, sum_over(): got = lax.all_to_all(sent, axis, 0, 0, tiled=True)  3.47 us
  transfers between devices with their start and end apart: 1, of which 0 were waited for; matrix products, arithmetic and copies ran while one was open for 0% of the time, Pallas kernels for 0%

profile of v1, /device:TPU:0, one launch (start us, length us, event | category | flops | bytes accessed | tf_op | source)
XLA Modules:
  0.0 81.4 jit_solution(9980370445225603771)
XLA Ops:
  0.6 0.0 copy-start
  0.6 0.0 copy-start.7
  0.7 6.9 %all_gather.9 = bf16[32,2048]{1,0:T(8,128)(2,1)S(1)} all-gather(bf16[32,512]{1,0:T(8,128)(2,1)} %param.17), channel_id=1, replica_groups=mesh['kv'=8,'tp'=4] {'tp'}, dimensions={1}, use_global_device_ids=true | all-gather | bytes 163840 | tf_op jit(solution)/shard_map/all_gather | solution.py:47
  7.5 0.1 fusion.12
  7.7 1.6 %convolution_convert_fusion.3 = bf16[32,256]{1,0:T(8,128)(2,1)S(1)} fusion(bf16[2048,256]{1,0:T(8,128)(2,1)} %param.22, bf16[32,2048]{1,0:T(8,128)(2,1)S(1)} %all_gather.9, f32[2048]{0:T(1024)} %param.21, f32[32]{0:T(128)S(1)} %add_rsqrt_fusion.1), kind=kOutput, calls=%fused_computation.13 | convolution fusion | flops 33824768 | bytes 1204352 | tf_op jit(solution)/shard_map/dot_general | solution.py:51
  9.3 0.7 dynamic_slice.10
  10.0 1.0 %fusion.19 = f32[32,2]{0,1:T(2,128)S(1)} fusion(f32[32,2]{0,1:T(2,128)} %param.20, bf16[2048,8]{0,1:T(8,128)(2,1)} %param.27, s32[]{:T(128)S(6)} %select_n.10, f32[2]{0:T(128)S(1)} %dynamic_slice.10, bf16[32,2048]{1,0:T(8,128)(2,1)S(1)} %all_gather.9, f32[2048]{0:T(1024)} %param.21, f32[32]{0:T(128)S(1)} %add_rsqrt_fusion.1), kind=kOutput, calls=%fused_computation.45 | convolution fusion | flops 524928 | bytes 148876 | tf_op jit(solution)/shard_map/dot_general | solution.py:62
  11.0 1.0 %broadcast_multiply_fusion.2 = (f32[32,2]{0,1:T(2,128)S(1)}, f32[32,2]{0,1:T(2,128)S(1)}, f32[32,2]{0,1:T(2,128)S(1)}) fusion(f32[32,2]{0,1:T(2,128)S(1)} %fusion.19, bf16[2048,8]{0,1:T(8,128)(2,1)} %param.26, s32[]{:T(128)S(6)} %select_n.10, bf16[32,2048]{1,0:T(8,128)(2,1)S(1)} %all_gather.9, f32[2048]{0:T(1024)} %param.21, f32[32]{0:T(128)S(1)} %add_rsqrt_fusion.1), kind=kOutput, calls=%fused_computation.49 | convolution fusion | flops 524480 | bytes 148612 | tf_op jit(solution)/shard_map/dot_general | solution.py:60
  12.0 0.0 copy-start.9
  12.0 0.1 copy.30
  12.1 0.1 copy.33
  12.2 0.1 copy.31
  12.3 1.6 %fusion.9 = f32[32,256]{1,0:T(8,128)S(1)} fusion(bf16[2048,256]{1,0:T(8,128)(2,1)} %param.24, bf16[32,2048]{1,0:T(8,128)(2,1)S(1)} %all_gather.9, f32[2048]{0:T(1024)} %param.21, f32[32]{0:T(128)S(1)} %add_rsqrt_fusion.1), kind=kOutput, calls=%fused_computation.17 | convolution fusion | flops 33832960 | bytes 1220736 | tf_op jit(solution)/shard_map/dot_general | solution.py:53
  13.9 1.6 %fusion.8 = f32[32,256]{1,0:T(8,128)S(1)} fusion(bf16[2048,256]{1,0:T(8,128)(2,1)} %param.23, bf16[32,2048]{1,0:T(8,128)(2,1)S(1)} %all_gather.9, f32[2048]{0:T(1024)} %param.21, f32[32]{0:T(128)S(1)} %add_rsqrt_fusion.1), kind=kOutput, calls=%fused_computation.15 | convolution fusion | flops 33832960 | bytes 1220736 | tf_op jit(solution)/shard_map/dot_general | solution.py:52
  15.5 0.0 copy-done.7
  15.5 0.8 multiply_reduce_fusion.1
  16.3 3.7 %multiply_add_fusion = f32[32,2,128,128]{3,2,1,0:T(8,128)S(1)} fusion(f32[32,2,128,128]{3,2,1,0:T(8,128)} %param.18, f32[32,2,128]{2,1,0:T(2,128)S(1)} %get-tuple-element.9, f32[32,2,128]{2,1,0:T(2,128)S(1)} %get-tuple-element.10, f32[32,2]{1,0:T(8,128)S(1)} %copy.30), kind=kLoop, calls=%fused_computation | loop fusion | flops 3145728 | bytes 8454400 | tf_op jit(solution)/shard_map/add | solution.py:71
  20.0 0.0 copy-done.9
  20.0 0.0 copy-start.1
  20.0 0.0 copy-start.4
  20.0 0.0 copy-start.5
  20.1 0.0 copy-start.10
  20.1 0.0 copy-start.3
  20.1 0.0 copy-start.6
  20.1 0.0 copy-start.8
  20.1 3.4 %fusion.30 = f32[32,2,1,128]{3,2,1,0:T(1,128)S(1)} fusion(f32[32,2,128,128]{3,2,1,0:T(8,128)S(1)} %multiply_add_fusion, bf16[32,2,128,1]{2,3,1,0:T(2,128)(2,1)S(1)} %reshape.83), kind=kOutput, calls=%fused_computation.53 | convolution fusion | flops 12582912 | bytes 4243456 | tf_op jit(solution)/shard_map/bhed,bhd->bhe/dot_general | solution.py:75
  23.5 0.1 broadcast_divide_fusion
  23.6 0.0 copy-done.4
  23.6 0.0 copy-done.5
  23.6 0.0 copy-done.10
  23.6 0.3 fusion.7
  24.0 5.4 %all_gather.10 = bf16[32,1024]{1,0:T(8,128)(2,1)S(1)} all-gather(bf16[32,256]{1,0:T(8,128)(2,1)S(1)} %fusion.7), channel_id=1, replica_groups=mesh['kv'=8,'tp'=4] {'tp'}, dimensions={1}, use_global_device_ids=true | all-gather | bytes 81920 | tf_op jit(solution)/shard_map/all_gather | solution.py:84
  29.4 0.0 copy-done.3
  29.4 0.0 copy-done.6
  29.4 0.0 copy-start.2
  29.4 0.3 fusion
  29.7 15.2 %all_to_all.15 = bf16[8,32,512]{2,1,0:T(8,128)(2,1)S(1)} all-to-all(bf16[8,32,512]{2,1,0:T(8,128)(2,1)S(1)} %broadcast_in_dim.2), channel_id=1, replica_groups=mesh['kv'=8,'tp'=4] {'kv'}, dimensions={0} | all-to-all | bytes 524288 | tf_op jit(solution)/shard_map/all_to_all | solution.py:90
  44.9 0.0 copy-done.8
  45.0 0.0 copy-done
  45.0 0.4 convolution_convert_fusion
  45.4 0.0 copy-done.1
  45.4 0.8 %copy.41 = bf16[32,4,8,256]{3,2,0,1:T(8,128)(2,1)} copy(bf16[32,4,8,256]{3,2,1,0:T(8,128)(2,1)S(1)} %bitcast.31) | data formatting | bytes 1048576 | tf_op jit(solution)/shard_map/reshape | solution.py:18
  46.3 3.5 %all-to-all-start.1 = ((bf16[4,256,256]{2,1,0:T(8,128)(2,1)}), bf16[4,256,256]{2,1,0:T(8,128)(2,1)S(1)}, u32[]{:S(2)}, u32[]{:S(2)}) async-start(bf16[4,256,256]{2,1,0:T(8,128)(2,1)} %bitcast.30), calls=%async_computation.1 | async-start | bytes 1048576 | tf_op jit(solution)/shard_map/all_to_all | solution.py:21
  49.7 0.1 multiply_reduce_fusion
  49.9 0.1 reduce_sum.51
  49.9 10.0 %psum.7 = f32[256]{0:T(256)S(1)} all-reduce(f32[256]{0:T(256)S(1)} %reduce_sum.51), channel_id=1, replica_groups=mesh['kv'=8,'tp'=4] {'tp'}, use_global_device_ids=true, to_apply=%region_4.5 | all-reduce | flops 256 | bytes 2048 | tf_op jit(solution)/shard_map/psum | solution.py:98
  60.0 0.0 all-to-all-done.1
  60.0 0.1 convert_reduce_fusion
  60.1 0.1 multiply_convert_fusion
  60.2 7.3 %all_gather.11 = bf16[256,1024]{1,0:T(8,128)(2,1)S(1)} all-gather(bf16[256,256]{1,0:T(8,128)(2,1)S(1)} %multiply_convert_fusion), channel_id=1, replica_groups=mesh['kv'=8,'tp'=4] {'tp'}, dimensions={1}, use_global_device_ids=true | all-gather | bytes 655360 | tf_op jit(solution)/shard_map/all_gather | solution.py:101
  67.5 0.0 copy-done.2
  67.5 0.4 convolution_convert_fusion.1
  67.9 12.8 %all_to_all.16 = bf16[8,32,512]{2,1,0:T(8,128)(2,1)S(1)} all-to-all(bf16[8,32,512]{2,1,0:T(8,128)(2,1)S(1)} %bitcast.32), channel_id=1, replica_groups=mesh['kv'=8,'tp'=4] {'kv'}, dimensions={0} | all-to-all | bytes 524288 | tf_op jit(solution)/shard_map/all_to_all | solution.py:21
  80.8 0.6 add_convert_fusion
  (11 shorter events, 0.2 us)
Async XLA Ops:
  0.6 44.3 %copy-start = (bf16[512,1024]{1,0:T(8,128)(2,1)S(1)}, bf16[512,1024]{1,0:T(8,128)(2,1)}, u32[]{:S(2)}) copy-start(bf16[512,1024]{1,0:T(8,128)(2,1)} %param.32) | copy-start | bytes 3145732
  0.6 14.9 %copy-start.7 = (f32[32,2,128]{2,1,0:T(2,128)S(1)}, f32[32,2,128]{2,1,0:T(2,128)}, u32[]{:S(2)}) copy-start(f32[32,2,128]{2,1,0:T(2,128)} %param.19) | copy-start | bytes 98308
  12.0 8.0 %copy-start.9 = (f32[32,2]{0,1:T(2,128)}, f32[32,2]{0,1:T(2,128)S(1)}, u32[]{:S(2)}) copy-start(f32[32,2]{0,1:T(2,128)S(1)} %get-tuple-element.8) | copy-start | bytes 772
  20.0 25.4 %copy-start.1 = (f32[32,2,128,128]{3,2,1,0:T(8,128)}, f32[32,2,128,128]{3,2,1,0:T(8,128)S(1)}, u32[]{:S(2)}) copy-start(f32[32,2,128,128]{3,2,1,0:T(8,128)S(1)} %multiply_add_fusion) | copy-start | bytes 12582916
  20.0 3.6 %copy-start.4 = (bf16[2048,256]{1,0:T(8,128)(2,1)S(1)}, bf16[2048,256]{1,0:T(8,128)(2,1)}, u32[]{:S(2)}) copy-start(bf16[2048,256]{1,0:T(8,128)(2,1)} %param.25) | copy-start | bytes 3145732
  20.0 3.6 %copy-start.5 = (f32[2048]{0:T(1024)S(1)}, f32[2048]{0:T(1024)}, u32[]{:S(2)}) copy-start(f32[2048]{0:T(1024)} %param.21) | copy-start | bytes 24580
  20.1 3.6 %copy-start.10 = (f32[256]{0:T(256)S(1)}, f32[256]{0:T(256)}, u32[]{:S(2)}) copy-start(f32[256]{0:T(256)} %param.29) | copy-start | bytes 3076
  20.1 9.3 %copy-start.3 = (bf16[1024,512]{1,0:T(8,128)(2,1)S(1)}, bf16[1024,512]{1,0:T(8,128)(2,1)}, u32[]{:S(2)}) copy-start(bf16[1024,512]{1,0:T(8,128)(2,1)} %param.30) | copy-start | bytes 3145732
  20.1 9.3 %copy-start.6 = (bf16[32,512]{1,0:T(8,128)(2,1)S(1)}, bf16[32,512]{1,0:T(8,128)(2,1)}, u32[]{:S(2)}) copy-start(bf16[32,512]{1,0:T(8,128)(2,1)} %param.17) | copy-start | bytes 98308
  20.1 24.8 %copy-start.8 = (f32[512]{0:T(512)S(1)}, f32[512]{0:T(512)}, u32[]{:S(2)}) copy-start(f32[512]{0:T(512)} %param.31) | copy-start | bytes 6148
  29.4 38.1 %copy-start.2 = (bf16[1024,512]{1,0:T(8,128)(2,1)S(1)}, bf16[1024,512]{1,0:T(8,128)(2,1)}, u32[]{:S(2)}) copy-start(bf16[1024,512]{1,0:T(8,128)(2,1)} %param.33) | copy-start | bytes 3145732
  46.3 13.7 %all-to-all-start.1 = ((bf16[4,256,256]{2,1,0:T(8,128)(2,1)}), bf16[4,256,256]{2,1,0:T(8,128)(2,1)S(1)}, u32[]{:S(2)}, u32[]{:S(2)}) async-start(bf16[4,256,256]{2,1,0:T(8,128)(2,1)} %bitcast.30), calls=%async_computation.1 | async-start | bytes 1048576 | tf_op jit(solution)/shard_map/all_to_all | solution.py:21

commit v2 on v1

v2 whole, which is shorter than its diff:
```python
import functools
import jax
import jax.numpy as jnp
from jax import lax
from jax.experimental import pallas as pl
from jax.experimental.pallas import tpu as pltpu
from jax.sharding import PartitionSpec as P

D = 2048
DK = 128
DV = 128


EPS = 1e-06


GROUP = 16


def cell_kernel(
    heads,
    *refs,
):
    blocks = lax.axis_size("tp")
    cell_body(heads, refs[:blocks], *refs[blocks:])


def cell_body(
    heads,
    rows_refs,
    gain_ref,
    query_ref,
    key_ref,
    value_ref,
    outgate_ref,
    input_ref,
    forget_ref,
    bias_ref,
    stabilizer_ref,
    normalizer_ref,
    memory_ref,
    memory_gain_ref,
    mixed_ref,
    normalizer_new_ref,
    stab_new_ref,
    keep_ref,
    admit_ref,
    keys_out_ref,
    values_out_ref,
):
    bf, f32 = jnp.bfloat16, jnp.float32
    first_head = lax.axis_index("tp") * heads
    me = lax.axis_index("tp")
    width = rows_refs[0].shape[1]
    squares = [jnp.square(ref[...].astype(f32)) for ref in rows_refs]
    squares = [jnp.sum(s, axis=-1, keepdims=True) for s in squares]
    scale_one = lax.rsqrt(sum(squares) / (width * len(squares)) + EPS)
    transposed = (((1,), (1,)), ((), ()))
    sums = [0.0] * 6
    for b, ref in enumerate(rows_refs):
        at = pl.ds(pl.multiple_of((me ^ b) * width, width), width)
        normed = (ref[...].astype(f32) * scale_one * gain_ref[:, at]).astype(bf)
        for n, w in enumerate((input_ref, forget_ref)):
            sums[n] += lax.dot_general(normed, w[:, at], transposed, preferred_element_type=f32)
        for n, w in enumerate((key_ref, query_ref, value_ref, outgate_ref)):
            sums[2 + n] += jnp.dot(normed, w[at, :], preferred_element_type=f32)
    input_all = sums[0]
    forget_all = jax.nn.log_sigmoid(sums[1] + bias_ref[...])
    keys, query, values, gate_out = (s.astype(bf) for s in sums[2:])
    keys_out_ref[...] = keys
    values_out_ref[...] = values
    lane = lax.broadcasted_iota(jnp.int32, input_all.shape, 1)
    count = rows_refs[0].shape[0]
    own = lax.broadcasted_iota(jnp.int32, keep_ref.shape, 1)
    diagonal = lax.broadcasted_iota(jnp.int32, (count, count), 0) == lax.broadcasted_iota(
        jnp.int32, (count, count), 1
    )
    keep_all, admit_all = (jnp.zeros(keep_ref.shape, f32) for _ in range(2))
    for h in range(heads):
        chosen = lane == first_head + h
        input_log = jnp.sum(jnp.where(chosen, input_all, 0.0), axis=1, keepdims=True)
        forget_log = jnp.sum(jnp.where(chosen, forget_all, 0.0), axis=1, keepdims=True)
        before = jnp.where(diagonal, stabilizer_ref[h : h + 1, :], 0.0)
        decayed = forget_log + jnp.sum(before, axis=1, keepdims=True)
        stab = jnp.maximum(decayed, input_log)
        keep = jnp.exp(decayed - stab)
        admit = jnp.exp(input_log - stab)
        stab_new_ref[h : h + 1, :] = jnp.sum(jnp.where(diagonal, stab, 0.0), axis=0, keepdims=True)
        keep_all = jnp.where(own == h, keep, keep_all)
        admit_all = jnp.where(own == h, admit, admit_all)
        cols = slice(h * DK, (h + 1) * DK)
        vcols = slice(h * DV, (h + 1) * DV)
        keys_f = keys[:, cols].astype(f32) * DK ** (-0.5)
        query_f = query[:, cols].astype(f32)
        normalizer_new = keep * normalizer_ref[:, h, :] + admit * keys_f
        normalizer_new_ref[:, h, :] = normalizer_new
        denom = jnp.sum(normalizer_new * query_f, axis=-1, keepdims=True)
        match = jnp.sum(keys_f * query_f, axis=-1, keepdims=True)
        groups = []
        for r in range(0, count, GROUP):
            some = query[r : r + GROUP, cols]
            place = lax.broadcasted_iota(jnp.int32, (GROUP, DV), 0)
            recalled = jnp.zeros((GROUP, DV), f32)
            for j in range(GROUP):
                stored = memory_ref[r + j, h].astype(bf)
                one = lax.dot_general(some, stored, transposed, preferred_element_type=f32)
                recalled = jnp.where(place == j, one, recalled)
            groups.append(recalled)
        recalled = jnp.concatenate(groups, axis=0)
        numer = keep * recalled + (admit * match) * values[:, vcols].astype(f32)
        cell = numer / jnp.maximum(jnp.abs(denom), 1.0)
        gate = jax.nn.sigmoid(gate_out[:, vcols].astype(f32))
        mixed_ref[:, vcols] = (cell * memory_gain_ref[:, vcols] * gate).astype(bf)
    keep_ref[...] = keep_all
    admit_ref[...] = admit_all


def fetch_kernel(count, *refs):
    copies = [
        pltpu.make_async_copy(refs[i], refs[count + i], refs[2 * count].at[i]) for i in range(count)
    ]
    for copy in copies:
        copy.start()
    for copy in copies:
        copy.wait()


def fetch(*args):
    args = [pltpu.with_memory_space_constraint(a, pltpu.HBM) for a in args]
    return pl.pallas_call(
        functools.partial(fetch_kernel, len(args)),
        out_shape=[pltpu.VMEM(a.shape, a.dtype) for a in args],
        in_specs=[pl.BlockSpec(memory_space=pltpu.HBM)] * len(args),
        out_specs=[pl.BlockSpec(memory_space=pltpu.VMEM)] * len(args),
        scratch_shapes=[pltpu.SemaphoreType.DMA((len(args),))],
        compiler_params=pltpu.CompilerParams(vmem_limit_bytes=2**20),
        cost_estimate=pl.CostEstimate(flops=10**9, bytes_accessed=9 * 2**20, transcendentals=0),
        name="fetch",
    )(*args)


def run_cell(blocks, heads, *args):
    own, f32 = blocks[0].shape[0], jnp.float32
    args = [pltpu.with_memory_space_constraint(a, pltpu.VMEM) for a in args]
    shapes = [
        ((own, heads * DV), jnp.bfloat16),
        ((own, heads, DK), f32),
        ((heads, own), f32),
        ((own, heads), f32),
        ((own, heads), f32),
        ((own, heads * DK), jnp.bfloat16),
        ((own, heads * DV), jnp.bfloat16),
    ]
    in_vmem = pl.BlockSpec(memory_space=pltpu.VMEM)
    return pl.pallas_call(
        functools.partial(cell_kernel, heads),
        out_shape=[jax.ShapeDtypeStruct(*s) for s in shapes],
        in_specs=[in_vmem] * (len(blocks) + len(args)),
        out_specs=[in_vmem] * len(shapes),
        compiler_params=pltpu.CompilerParams(vmem_limit_bytes=8 * 2**20),
        cost_estimate=pl.CostEstimate(flops=10**9, bytes_accessed=9 * 2**20, transcendentals=0),
        name="cell",
    )(*blocks, *args)


def swap(array, bit):
    pairs = [(i, i ^ bit) for i in range(lax.axis_size("tp"))]
    return lax.ppermute(array, "tp", pairs)


def per_device(
    tokens,
    memory,
    normalizer,
    stabilizer,
    norm_gain,
    query_weight,
    key_weight,
    value_weight,
    outgate_weight,
    input_gate_weight,
    forget_gate_weight,
    forget_bias,
    memory_gain,
    proj_weight,
    ffn_gain,
    up_weight,
    down_weight,
):
    own_rows = tokens.shape[0]
    heads_here = memory.shape[1]
    blocks = [tokens] + [swap(tokens, b) for b in reversed(range(1, lax.axis_size("tp")))][::-1]
    held = fetch(
        norm_gain.reshape(1, -1),
        query_weight,
        key_weight,
        value_weight,
        outgate_weight,
        input_gate_weight.T,
        forget_gate_weight.T,
        forget_bias.reshape(1, -1),
        stabilizer.T,
        normalizer,
        memory,
        memory_gain.reshape(1, -1),
    )
    mixed, normalizer_new, stab_new, keep, admit, keys, values = run_cell(blocks, heads_here, *held)
    stab_new = stab_new.T
    projected = jnp.dot(
        lax.all_gather(mixed, "tp", axis=1, tiled=True),
        proj_weight,
        preferred_element_type=jnp.float32,
    )
    second = (tokens.astype(jnp.float32) + projected).astype(jnp.bfloat16)
    second, keep, admit, keys, values = lax.optimization_barrier(
        (second, keep, admit, keys, values)
    )
    keys_f = keys.astype(jnp.float32).reshape(own_rows, heads_here, DK) * DK ** (-0.5)
    values_f = values.astype(jnp.float32).reshape(own_rows, heads_here, DV)
    memory_new = (
        keep[..., None, None] * memory
        + admit[..., None, None] * values_f[..., :, None] * keys_f[..., None, :]
    )
    groups = lax.axis_size("kv")
    all_rows = lax.all_to_all(
        jnp.broadcast_to(second, (groups,) + second.shape), "kv", 0, 0, tiled=True
    ).reshape(groups * own_rows, second.shape[1])
    scaled = (all_rows.astype(jnp.float32) * ffn_gain).astype(jnp.bfloat16)
    half = up_weight.shape[1] // 2
    side = lax.axis_index("tp") % 2
    mine, theirs = side * half, (1 - side) * half
    up_mine = lax.dynamic_slice_in_dim(up_weight, mine, half, 1)
    up_theirs = lax.dynamic_slice_in_dim(up_weight, theirs, half, 1)
    away = jnp.dot(scaled, up_theirs, preferred_element_type=jnp.float32).astype(jnp.bfloat16)
    came = swap(away, 1)
    preact = jnp.dot(scaled, up_mine, preferred_element_type=jnp.float32) + came.astype(jnp.float32)
    second_f = second.astype(jnp.float32)
    square_sum = jnp.sum(second_f * second_f, axis=-1, keepdims=True)
    square_sum = square_sum + swap(square_sum, 1)
    bit = 2
    while bit < lax.axis_size("tp"):
        sent = preact.astype(jnp.bfloat16)
        preact = sent.astype(jnp.float32) + swap(sent, bit).astype(jnp.float32)
        square_sum = square_sum + swap(square_sum, bit)
        bit *= 2
    hidden = jnp.square(jax.nn.relu(preact)).astype(jnp.bfloat16)
    other = swap(hidden, 1)
    down_mine = lax.dynamic_slice_in_dim(down_weight, mine, half, 0)
    down_theirs = lax.dynamic_slice_in_dim(down_weight, theirs, half, 0)
    partial = jnp.dot(hidden, down_mine, preferred_element_type=jnp.float32)
    partial = partial + jnp.dot(other, down_theirs, preferred_element_type=jnp.float32)
    sent = partial.astype(jnp.bfloat16).reshape(groups, own_rows, -1)
    got = lax.all_to_all(sent, "kv", 0, 0, tiled=True)
    summed = jnp.sum(got.astype(jnp.float32), axis=0)
    scale_two = lax.rsqrt(square_sum / D + EPS)
    layer_out = (second_f + summed * (scale_two * scale_two)).astype(jnp.bfloat16)
    return (layer_out, memory_new, normalizer_new, stab_new)


def solution(mesh):
    placed = (
        P("kv", "tp"),
        P("kv", "tp", None, None),
        P("kv", "tp", None),
        P("kv", "tp"),
        P(),
        P(None, "tp"),
        P(None, "tp"),
        P(None, "tp"),
        P(None, "tp"),
        P(),
        P(),
        P(),
        P("tp"),
        P(None, "tp"),
        P("tp"),
        P("tp", "kv"),
        P("kv", "tp"),
    )
    return jax.shard_map(
        per_device,
        mesh=mesh,
        in_specs=placed,
        out_specs=(P("kv", "tp"), P("kv", "tp", None, None), P("kv", "tp", None), P("kv", "tp")),
        check_vma=False,
    )
```

time: 82 us -> 59.8 us (0.73)
  blocking collectives: 57.7 us -> 5.41 us
  waiting for transfers between devices: 0.01 us -> 22.4 us
  starting transfers between devices: 3.47 us -> 16.1 us
  matrix products: 11.5 us -> 2.19 us
  Pallas kernels: 0 us -> 6.26 us
  local copies, waits for them, and re-layouts: 2.06 us -> 0.81 us
    all_to_all x2 -> x0, blocking collectives: 28 us -> none  [the longest x1 15.2 us: per_device(): lax.all_to_all(jnp.broadcast_to(second, (groups,) + second.shape), 'kv',...]
    all_to_all x1 -> x2, waiting for transfers between devices: 0.01 us -> 14.4 us  [the longest x1 9.43 us: per_device(): lax.all_to_all(jnp.broadcast_to(second, (groups,) + second.shape), 'kv',...]
    all_gather x2 -> x0, blocking collectives: 14.2 us -> none  [the longest x1 7.32 us: per_device(): hidden = lax.all_gather(partial_hidden, 'tp', axis=1, tiled=True)]
    psum x1 -> x0, blocking collectives: 10 us -> none  [per_device(): square_sum = lax.psum(square_sum, 'tp')]
    dot_general x9 -> x4, matrix products: 11.3 us -> 1.92 us  [the longest x1 1.01 us: per_device(): jnp.dot(other, down_theirs, preferred_element_type=jnp.float32)]
    ppermute x0 -> x8, waiting for transfers between devices: none -> 7.99 us  [swap(): return lax.ppermute(array, 'tp', pairs)]
    ppermute x0 -> x8, starting transfers between devices: none -> 6.56 us  [swap(): return lax.ppermute(array, 'tp', pairs)]
    pallas_call x0 -> x2, Pallas kernels: none -> 6.26 us  [the longest x1 3.64 us: fetch(): pl.pallas_call(functools.partial(fetch_kernel, len(args)), out_shape=[plt...]
  transfers between devices with their start and end apart: 1 -> 10, of which waited for: 0 -> 4; matrix products, arithmetic and copies ran while one was open for 0% -> 10% of each run, Pallas kernels for 0% -> 6%
where the time goes in v2:
time: 59.8 us; the launch traced here: 59.4 us
  waiting for transfers between devices  22.4 us (37%)
  starting transfers between devices  16.1 us (27%)
  Pallas kernels  6.26 us (10%)
  other arithmetic  5.43 us (9%)
  blocking collectives  5.41 us (9%)
  matrix products  2.19 us (4%)
  between operations  0.84 us (1%)
  local copies, waits for them, and re-layouts  0.81 us (1%)
    all_to_all x1, waiting for transfers between devices, per_device(): lax.all_to_all(jnp.broadcast_to(second, (groups,) + second.shape), 'kv',...  9.43 us
    ppermute x8, waiting for transfers between devices, swap(): return lax.ppermute(array, 'tp', pairs)  7.99 us
    ppermute x8, starting transfers between devices, swap(): return lax.ppermute(array, 'tp', pairs)  6.56 us
    all_to_all x1, starting transfers between devices, per_device(): lax.all_to_all(jnp.broadcast_to(second, (groups,) + second.shape), 'kv',...  5.98 us
    all_gather x1, blocking collectives, per_device(): lax.all_gather(mixed, 'tp', axis=1, tiled=True)  5.41 us
    all_to_all x1, waiting for transfers between devices, per_device(): got = lax.all_to_all(sent, 'kv', 0, 0, tiled=True)  4.94 us
    add x1, other arithmetic, per_device(): keep[..., None, None] * memory  4.31 us
    pallas_call x1, Pallas kernels, fetch(): pl.pallas_call(functools.partial(fetch_kernel, len(args)), out_shape=[plt...  3.64 us
  transfers between devices with their start and end apart: 10, of which 4 were waited for; matrix products, arithmetic and copies ran while one was open for 10% of the time, Pallas kernels for 6%

profile of v2, /device:TPU:0, one launch (start us, length us, event | category | flops | bytes accessed | tf_op | source)
XLA Modules:
  0.0 59.4 jit_solution(6650747976789964074)
XLA Ops:
  0.6 0.0 copy-start
  0.7 0.6 collective-permute-start
  1.2 2.6 %collective-permute-start.1 = (bf16[32,512]{1,0:T(8,128)(2,1)}, bf16[32,512]{1,0:T(8,128)(2,1)S(1)}, u32[]{:S(2)}, u32[]{:S(2)}) collective-permute-start(bf16[32,512]{1,0:T(8,128)(2,1)} %refs_0_.1), channel_id=1, source_target_pairs={{0,2},{1,3},{2,0},{3,1},{4,6},{5,7},{6,4},{7,5},{8,10},{9,11},{10,... | collective-permute-start | bytes 98312 | tf_op jit(solution)/shard_map/ppermute | solution.py:168
  3.8 0.0 collective-permute-start.2
  3.8 0.0 copy-start.1
  3.8 3.6 %fetch.1 = (f32[1,2048]{1,0:T(1,128)S(1)}, bf16[2048,256]{1,0:T(8,128)(2,1)S(1)}, bf16[2048,256]{1,0:T(8,128)(2,1)S(1)}, bf16[2048,256]{1,0:T(8,128)(2,1)S(1)}, ...) custom-call(f32[1,2048]{1,0:T(1,128)} %bitcast.23, ...), custom_call_target="tpu_custom_call" | custom-call | flops 1000000000 | bytes 9437184 | tf_op jit(solution)/shard_map/fetch/pallas_call | solution.py:130
  7.5 0.0 collective-permute-done.refs_1_
  7.5 0.0 collective-permute-done.1.refs_2_
  7.5 0.0 collective-permute-done.2.refs_3_
  7.5 0.0 copy-done.1
  7.5 0.0 copy-start.3
  7.5 0.0 copy-start.4
  7.5 2.6 %cell.1 = (bf16[32,256]{1,0:T(8,128)(2,1)S(1)}, f32[32,2,128]{2,1,0:T(2,128)}, f32[2,32]{1,0:T(2,128)}, f32[32,2]{1,0:T(8,128)S(1)}, f32[32,2]{1,0:T(8,128)S(1)}...) custom-call(bf16[32,512]{1,0:T(8,128)(2,1)S(1)} %copy-done.1, ...), custom_call_target="tpu_custom_call" | custom-call | flops 1000000000 | bytes 9437184 | tf_op jit(solution)/shard_map/cell/pallas_call | solution.py:155
  10.2 0.0 copy-start.2
  10.2 5.4 %all_gather.3 = bf16[32,1024]{1,0:T(8,128)(2,1)S(1)} all-gather(bf16[32,256]{1,0:T(8,128)(2,1)S(1)} %get-tuple-element.40), channel_id=1, replica_groups=mesh['kv'=8,'tp'=4] {'tp'}, dimensions={1}, use_global_device_ids=true | all-gather | bytes 81920 | tf_op jit(solution)/shard_map/all_gather | solution.py:210
  15.6 0.0 copy-done.3
  15.6 0.3 fusion.1
  15.9 0.7 %broadcast_in_dim.4 = bf16[8,32,512]{2,1,0:T(8,128)(2,1)} broadcast(bf16[32,512]{1,0:T(8,128)(2,1)S(1)} %fusion.1), dimensions={1,2} | broadcast | bytes 294912 | tf_op jit(solution)/shard_map/broadcast_in_dim | solution.py:226
  16.6 6.0 %all-to-all-start = ((bf16[8,32,512]{2,1,0:T(8,128)(2,1)}), bf16[8,32,512]{2,1,0:T(8,128)(2,1)S(1)}, u32[]{:S(2)}, u32[]{:S(2)}) async-start(bf16[8,32,512]{2,1,0:T(8,128)(2,1)} %broadcast_in_dim.4), calls=%async_computation | async-start | bytes 524288 | tf_op jit(solution)/shard_map/all_to_all | solution.py:225
  22.6 9.4 %all-to-all-done = bf16[8,32,512]{2,1,0:T(8,128)(2,1)S(1)} async-done(((bf16[8,32,512]{2,1,0:T(8,128)(2,1)}), bf16[8,32,512]{2,1,0:T(8,128)(2,1)S(1)}, u32[]{:S(2)}, u32[]{:S(2)}) %all-to-all-start) | async-done | bytes 262176 | tf_op jit(solution)/shard_map/all_to_all | solution.py:225
  32.0 0.0 copy-done.4
  32.0 0.1 fusion.2
  32.1 0.0 copy-done
  32.1 0.3 convolution_convert_fusion
  32.4 0.1 collective-permute-start.3
  32.5 1.5 %collective-permute-done.3 = bf16[256,512]{1,0:T(8,128)(2,1)S(1)} collective-permute-done((bf16[256,512]{1,0:T(8,128)(2,1)S(1)}, bf16[256,512]{1,0:T(8,128)(2,1)S(1)}, u32[]{:S(2)}, u32[]{:S(2)}) %collective-permute-start.3) | collective-permute-done | bytes 262176 | tf_op jit(solution)/shard_map/ppermute | solution.py:168
  34.0 0.3 add_convert_fusion
  34.3 1.6 %collective-permute-start.4 = (bf16[256,512]{1,0:T(8,128)(2,1)S(1)}, bf16[256,512]{1,0:T(8,128)(2,1)S(1)}, u32[]{:S(2)}, u32[]{:S(2)}) collective-permute-start(bf16[256,512]{1,0:T(8,128)(2,1)S(1)} %add_convert_fusion), channel_id=1, source_target_pairs={{0,2},{1,3},{2,0},{3,1},{4,6},{5,7},{6,4},{7,5},{8,10},{9,11},{10,... | collective-permute-start | bytes 786440 | tf_op jit(solution)/shard_map/ppermute | solution.py:168
  35.9 0.1 fusion.11
  36.1 0.1 collective-permute-start.6
  36.1 0.1 broadcast_multiply_fusion
  36.2 6.5 %collective-permute-done.4 = bf16[256,512]{1,0:T(8,128)(2,1)S(1)} collective-permute-done((bf16[256,512]{1,0:T(8,128)(2,1)S(1)}, bf16[256,512]{1,0:T(8,128)(2,1)S(1)}, u32[]{:S(2)}, u32[]{:S(2)}) %collective-permute-start.4) | collective-permute-done | bytes 262176 | tf_op jit(solution)/shard_map/ppermute | solution.py:168
  42.7 0.1 multiply_convert_fusion
  42.8 0.1 collective-permute-start.5
  42.9 0.0 collective-permute-done.6
  42.9 1.6 %collective-permute-start.7 = (f32[32,1]{0,1:T(1,128)S(1)}, f32[32,1]{0,1:T(1,128)S(1)}, u32[]{:S(2)}, u32[]{:S(2)}) collective-permute-start(f32[32,1]{0,1:T(1,128)S(1)} %bitcast_add_fusion), channel_id=1, source_target_pairs={{0,2},{1,3},{2,0},{3,1},{4,6},{5,7},{6,4},{7,5},{8,10},{9,11},{10,... | collective-permute-start | bytes 392 | tf_op jit(solution)/shard_map/ppermute | solution.py:168
  44.5 0.0 copy-done.2
  44.5 0.3 fusion.4
  44.8 0.0 collective-permute-done.5
  44.8 1.0 %fusion = bf16[256,512]{1,0:T(8,128)(2,1)} fusion(f32[256,512]{1,0:T(8,128)S(1)} %fusion.4, bf16[256,512]{1,0:T(8,128)(2,1)S(1)} %collective-permute-done.5, bf16[1024,512]{1,0:T(8,128)(2,1)S(1)} %copy-done.2, s32[]{:T(128)S(6)} %select_n.17), kind=kOutput, calls=%fused_computation.2 | convolution fusion | flops 134479872 | bytes 1572868 | tf_op jit(solution)/shard_map/dot_general | solution.py:251
  45.8 3.6 %all-to-all-start.1 = ((bf16[8,32,512]{2,1,0:T(8,128)(2,1)}), bf16[8,32,512]{2,1,0:T(8,128)(2,1)S(1)}, u32[]{:S(2)}, u32[]{:S(2)}) async-start(bf16[8,32,512]{2,1,0:T(8,128)(2,1)} %bitcast.7), calls=%async_computation.1 | async-start | bytes 524288 | tf_op jit(solution)/shard_map/all_to_all | solution.py:253
  49.4 4.3 %multiply_add_fusion = f32[32,2,128,128]{3,2,1,0:T(8,128)} fusion(f32[32,2,128,128]{3,2,1,0:T(8,128)} %refs_10_.1, f32[32,2,128]{2,1,0:T(2,128)S(1)} %mul.93, f32[32,2,128]{2,1,0:T(2,128)S(1)} %broadcast_multiply_fusion, f32[32,2]{1,0:T(8,128)S(1)} %get-tuple-element.46), kind=kLoop, calls=%fused_computation | loop fusion | flops 3145728 | bytes 8454400 | tf_op jit(solution)/shard_map/add | solution.py:221
  53.7 0.0 collective-permute-done.7
  53.7 4.9 %all-to-all-done.1 = bf16[8,32,512]{2,1,0:T(8,128)(2,1)S(1)} async-done(((bf16[8,32,512]{2,1,0:T(8,128)(2,1)}), bf16[8,32,512]{2,1,0:T(8,128)(2,1)S(1)}, u32[]{:S(2)}, u32[]{:S(2)}) %all-to-all-start.1) | async-done | bytes 262176 | tf_op jit(solution)/shard_map/all_to_all | solution.py:253
  58.7 0.7 %fusion.12 = bf16[32,512]{1,0:T(8,128)(2,1)} fusion(bf16[32,512]{1,0:T(8,128)(2,1)S(1)} %fusion.1, f32[32,512]{1,0:T(8,128)S(1)} %convert_reduce_fusion, f32[32]{0:T(128)S(1)} %multiply_bitcast_fusion), kind=kLoop, calls=%fused_computation.20 | loop fusion | flops 65536 | bytes 131200 | tf_op jit(solution)/shard_map/convert_element_type | solution.py:256
  (6 shorter events, 0.1 us)
Async XLA Ops:
  0.6 31.4 %copy-start = (bf16[512,1024]{1,0:T(8,128)(2,1)S(1)}, bf16[512,1024]{1,0:T(8,128)(2,1)}, u32[]{:S(2)}) copy-start(bf16[512,1024]{1,0:T(8,128)(2,1)} %param.32) | copy-start | bytes 3145732
  0.7 6.8 %collective-permute-start = (bf16[32,512]{1,0:T(8,128)(2,1)}, bf16[32,512]{1,0:T(8,128)(2,1)S(1)}, u32[]{:S(2)}, u32[]{:S(2)}) collective-permute-start(bf16[32,512]{1,0:T(8,128)(2,1)} %refs_0_.1), channel_id=1, source_target_pairs={{0,1},{1,0},{2,3},{3,2},{4,5},{5,4},{6,7},{7,6},{8,9},{9,8},{10,11... | collective-permute-start | bytes 98312 | tf_op jit(solution)/shard_map/ppermute | solution.py:168
  1.2 6.3 %collective-permute-start.1 = (bf16[32,512]{1,0:T(8,128)(2,1)}, bf16[32,512]{1,0:T(8,128)(2,1)S(1)}, u32[]{:S(2)}, u32[]{:S(2)}) collective-permute-start(bf16[32,512]{1,0:T(8,128)(2,1)} %refs_0_.1), channel_id=1, source_target_pairs={{0,2},{1,3},{2,0},{3,1},{4,6},{5,7},{6,4},{7,5},{8,10},{9,11},{10,... | collective-permute-start | bytes 98312 | tf_op jit(solution)/shard_map/ppermute | solution.py:168
  3.8 3.7 %collective-permute-start.2 = (bf16[32,512]{1,0:T(8,128)(2,1)}, bf16[32,512]{1,0:T(8,128)(2,1)S(1)}, u32[]{:S(2)}, u32[]{:S(2)}) collective-permute-start(bf16[32,512]{1,0:T(8,128)(2,1)} %refs_0_.1), channel_id=1, source_target_pairs={{0,3},{1,2},{2,1},{3,0},{4,7},{5,6},{6,5},{7,4},{8,11},{9,10},{10,... | collective-permute-start | bytes 98312 | tf_op jit(solution)/shard_map/ppermute | solution.py:168
  3.8 3.7 %copy-start.1 = (bf16[32,512]{1,0:T(8,128)(2,1)S(1)}, bf16[32,512]{1,0:T(8,128)(2,1)}, u32[]{:S(2)}) copy-start(bf16[32,512]{1,0:T(8,128)(2,1)} %refs_0_.1) | copy-start | bytes 98308
  7.5 8.1 %copy-start.3 = (bf16[1024,512]{1,0:T(8,128)(2,1)S(1)}, bf16[1024,512]{1,0:T(8,128)(2,1)}, u32[]{:S(2)}) copy-start(bf16[1024,512]{1,0:T(8,128)(2,1)} %param.30) | copy-start | bytes 3145732
  7.5 24.5 %copy-start.4 = (f32[512]{0:T(512)S(1)}, f32[512]{0:T(512)}, u32[]{:S(2)}) copy-start(f32[512]{0:T(512)} %param.31) | copy-start | bytes 6148
  10.2 34.3 %copy-start.2 = (bf16[1024,512]{1,0:T(8,128)(2,1)S(1)}, bf16[1024,512]{1,0:T(8,128)(2,1)}, u32[]{:S(2)}) copy-start(bf16[1024,512]{1,0:T(8,128)(2,1)} %param.33) | copy-start | bytes 3145732
  16.6 15.4 %all-to-all-start = ((bf16[8,32,512]{2,1,0:T(8,128)(2,1)}), bf16[8,32,512]{2,1,0:T(8,128)(2,1)S(1)}, u32[]{:S(2)}, u32[]{:S(2)}) async-start(bf16[8,32,512]{2,1,0:T(8,128)(2,1)} %broadcast_in_dim.4), calls=%async_computation | async-start | bytes 524288 | tf_op jit(solution)/shard_map/all_to_all | solution.py:225
  32.4 1.6 %collective-permute-start.3 = (bf16[256,512]{1,0:T(8,128)(2,1)S(1)}, bf16[256,512]{1,0:T(8,128)(2,1)S(1)}, u32[]{:S(2)}, u32[]{:S(2)}) collective-permute-start(bf16[256,512]{1,0:T(8,128)(2,1)S(1)} %convolution_convert_fusion), channel_id=1, source_target_pairs={{0,1},{1,0},{2,3},{3,2},{4,5},{5,4},{6,7},{7,6},{8,9},{9,8},{10,11... | collective-permute-start | bytes 786440 | tf_op jit(solution)/shard_map/ppermute | solution.py:168
  34.3 8.4 %collective-permute-start.4 = (bf16[256,512]{1,0:T(8,128)(2,1)S(1)}, bf16[256,512]{1,0:T(8,128)(2,1)S(1)}, u32[]{:S(2)}, u32[]{:S(2)}) collective-permute-start(bf16[256,512]{1,0:T(8,128)(2,1)S(1)} %add_convert_fusion), channel_id=1, source_target_pairs={{0,2},{1,3},{2,0},{3,1},{4,6},{5,7},{6,4},{7,5},{8,10},{9,11},{10,... | collective-permute-start | bytes 786440 | tf_op jit(solution)/shard_map/ppermute | solution.py:168
  36.1 6.8 %collective-permute-start.6 = (f32[32,1]{0,1:T(1,128)S(1)}, f32[32,1]{0,1:T(1,128)S(1)}, u32[]{:S(2)}, u32[]{:S(2)}) collective-permute-start(f32[32,1]{0,1:T(1,128)S(1)} %bitcast.27), channel_id=1, source_target_pairs={{0,1},{1,0},{2,3},{3,2},{4,5},{5,4},{6,7},{7,6},{8,9},{9,8},{10,11... | collective-permute-start | bytes 392 | tf_op jit(solution)/shard_map/ppermute | solution.py:168
  42.8 2.0 %collective-permute-start.5 = (bf16[256,512]{1,0:T(8,128)(2,1)S(1)}, bf16[256,512]{1,0:T(8,128)(2,1)S(1)}, u32[]{:S(2)}, u32[]{:S(2)}) collective-permute-start(bf16[256,512]{1,0:T(8,128)(2,1)S(1)} %multiply_convert_fusion), channel_id=1, source_target_pairs={{0,1},{1,0},{2,3},{3,2},{4,5},{5,4},{6,7},{7,6},{8,9},{9,8},{10,11... | collective-permute-start | bytes 786440 | tf_op jit(solution)/shard_map/ppermute | solution.py:168
  42.9 10.8 %collective-permute-start.7 = (f32[32,1]{0,1:T(1,128)S(1)}, f32[32,1]{0,1:T(1,128)S(1)}, u32[]{:S(2)}, u32[]{:S(2)}) collective-permute-start(f32[32,1]{0,1:T(1,128)S(1)} %bitcast_add_fusion), channel_id=1, source_target_pairs={{0,2},{1,3},{2,0},{3,1},{4,6},{5,7},{6,4},{7,5},{8,10},{9,11},{10,... | collective-permute-start | bytes 392 | tf_op jit(solution)/shard_map/ppermute | solution.py:168
  45.8 12.9 %all-to-all-start.1 = ((bf16[8,32,512]{2,1,0:T(8,128)(2,1)}), bf16[8,32,512]{2,1,0:T(8,128)(2,1)S(1)}, u32[]{:S(2)}, u32[]{:S(2)}) async-start(bf16[8,32,512]{2,1,0:T(8,128)(2,1)} %bitcast.7), calls=%async_computation.1 | async-start | bytes 524288 | tf_op jit(solution)/shard_map/all_to_all | solution.py:253

commit v3 on v2

--- a/solution.py
+++ b/solution.py
@@ -15,6 +15,7 @@
 
 
 GROUP = 16
+CHUNKS = 2
 
 
 def cell_kernel(
@@ -163,6 +164,178 @@
     )(*blocks, *args)
 
 
+STEP = 4
+
+
+def update_kernel(
+    memory_ref,
+    keep_ref,
+    admit_ref,
+    keys_ref,
+    values_ref,
+    proj_ref,
+    out_ref,
+    held_ref,
+    staged_ref,
+    sems,
+    held_sem,
+):
+    f32 = jnp.float32
+    rows, heads = memory_ref.shape[:2]
+    held = pltpu.make_async_copy(proj_ref, held_ref, held_sem)
+    held.start()
+    values = values_ref[...].astype(f32)
+    values = jnp.concatenate([values, jnp.zeros((128 - rows, values.shape[1]), f32)], axis=0)
+    columns = [jnp.transpose(values[:, h * DV : (h + 1) * DV]) for h in range(heads)]
+    keys = keys_ref[...].astype(f32) * DK ** (-0.5)
+    copies = []
+    for r in range(rows):
+        for h in range(heads):
+            key = keys[r : r + 1, h * DK : (h + 1) * DK] * admit_ref[r : r + 1, h : h + 1]
+            added = columns[h][:, r : r + 1] * key
+            staged_ref[r, h] = keep_ref[r : r + 1, h : h + 1] * memory_ref[r, h] + added
+        if r % STEP == STEP - 1:
+            part = pl.ds(r - STEP + 1, STEP)
+            copy = pltpu.make_async_copy(staged_ref.at[part], out_ref.at[part], sems.at[r // STEP])
+            copy.start()
+            copies.append(copy)
+    for copy in copies:
+        copy.wait()
+    held.wait()
+
+
+def run_update(memory, keep, admit, keys, values, proj):
+    in_vmem = pl.BlockSpec(memory_space=pltpu.VMEM)
+    args = [pltpu.with_memory_space_constraint(a, pltpu.VMEM) for a in (memory, keep, admit, keys, values)]
+    args.append(pltpu.with_memory_space_constraint(proj, pltpu.HBM))
+    return pl.pallas_call(
+        update_kernel,
+        out_shape=[
+            pltpu.HBM(memory.shape, memory.dtype),
+            pltpu.VMEM(proj.shape, proj.dtype),
+        ],
+        in_specs=[in_vmem] * 5 + [pl.BlockSpec(memory_space=pltpu.HBM)],
+        out_specs=[pl.BlockSpec(memory_space=pltpu.HBM), in_vmem],
+        scratch_shapes=[
+            pltpu.VMEM(memory.shape, memory.dtype),
+            pltpu.SemaphoreType.DMA((memory.shape[0] // STEP,)),
+            pltpu.SemaphoreType.DMA,
+        ],
+        compiler_params=pltpu.CompilerParams(vmem_limit_bytes=12 * 2**20),
+        cost_estimate=pl.CostEstimate(flops=10**9, bytes_accessed=9 * 2**20, transcendentals=0),
+        name="update",
+    )(*args)
+
+
+def second_kernel(*refs):
+    blocks = lax.axis_size("tp")
+    proj_ref, tokens_ref, sent_ref, second_ref, square_ref = refs[blocks:]
+    f32 = jnp.float32
+    width = refs[0].shape[1]
+    me = lax.axis_index("tp")
+    total = tokens_ref[...].astype(f32)
+    for b in range(blocks):
+        at = pl.ds(pl.multiple_of((me ^ b) * width, width), width)
+        total += jnp.dot(refs[b][...], proj_ref[at, :], preferred_element_type=f32)
+    second = total.astype(jnp.bfloat16)
+    second_ref[...] = second
+    for i in range(sent_ref.shape[0]):
+        sent_ref[i] = second
+    second = second.astype(f32)
+    square_ref[...] = jnp.sum(second * second, axis=1, keepdims=True)
+
+
+def run_second(blocks, proj, tokens, copies):
+    in_vmem = pl.BlockSpec(memory_space=pltpu.VMEM)
+    args = [pltpu.with_memory_space_constraint(a, pltpu.VMEM) for a in (*blocks, proj, tokens)]
+    return pl.pallas_call(
+        second_kernel,
+        out_shape=[
+            jax.ShapeDtypeStruct((copies,) + tokens.shape, jnp.bfloat16),
+            jax.ShapeDtypeStruct(tokens.shape, jnp.bfloat16),
+            jax.ShapeDtypeStruct((tokens.shape[0], 1), jnp.float32),
+        ],
+        in_specs=[in_vmem] * len(args),
+        out_specs=[in_vmem] * 3,
+        compiler_params=pltpu.CompilerParams(vmem_limit_bytes=4 * 2**20),
+        cost_estimate=pl.CostEstimate(flops=10**8, bytes_accessed=2**21, transcendentals=0),
+        name="second",
+    )(*args)
+
+
+def up_kernel(rows_ref, gain_ref, up_ref, *out_refs):
+    f32 = jnp.float32
+    side = lax.axis_index("tp") & 1
+    half = up_ref.shape[1] // 2
+    own, theirs = (pl.ds(pl.multiple_of(s * half, half), half) for s in (side, 1 - side))
+    groups = rows_ref.shape[0] // CHUNKS
+    for c in range(CHUNKS):
+        rows = rows_ref[c * groups : (c + 1) * groups].astype(f32) * gain_ref[...]
+        rows = rows.reshape(-1, rows.shape[-1]).astype(jnp.bfloat16)
+        away = jnp.dot(rows, up_ref[:, theirs], preferred_element_type=f32)
+        out_refs[c][...] = away.astype(jnp.bfloat16)
+        out_refs[CHUNKS + c][...] = jnp.dot(rows, up_ref[:, own], preferred_element_type=f32)
+
+
+def run_up(rows, gain, up):
+    in_vmem = pl.BlockSpec(memory_space=pltpu.VMEM)
+    shape = (rows.shape[0] * rows.shape[1] // CHUNKS, up.shape[1] // 2)
+    outs = pl.pallas_call(
+        up_kernel,
+        out_shape=[jax.ShapeDtypeStruct(shape, jnp.bfloat16)] * CHUNKS
+        + [jax.ShapeDtypeStruct(shape, jnp.float32)] * CHUNKS,
+        in_specs=[in_vmem] * 3,
+        out_specs=[in_vmem] * (2 * CHUNKS),
+        compiler_params=pltpu.CompilerParams(vmem_limit_bytes=8 * 2**20),
+        cost_estimate=pl.CostEstimate(flops=10**9, bytes_accessed=2**21, transcendentals=0),
+        name="up",
+    )(rows, gain, up)
+    return outs[:CHUNKS], outs[CHUNKS:]
+
+
+def halves(down_ref):
+    side = lax.axis_index("tp") & 1
+    half = down_ref.shape[0] // 2
+    return (down_ref[pl.ds(pl.multiple_of(s * half, half), half), :] for s in (side, 1 - side))
+
+
+def down_kernel(*refs):
+    f32 = jnp.float32
+    *inputs, down_ref, out_ref = refs
+    hidden, other = inputs[:CHUNKS], inputs[CHUNKS:]
+    own, theirs = halves(down_ref)
+    step = hidden[0].shape[0]
+    for c in range(CHUNKS):
+        total = jnp.dot(hidden[c][...], own, preferred_element_type=f32)
+        if c < len(other):
+            total += jnp.dot(other[c][...], theirs, preferred_element_type=f32)
+        out_ref[c * step : (c + 1) * step, :] = total
+
+
+def last_kernel(partial_ref, other_ref, down_ref, out_ref):
+    _, theirs = halves(down_ref)
+    begin = partial_ref.shape[0] - other_ref.shape[0]
+    last = partial_ref[begin:, :]
+    last += jnp.dot(other_ref[...], theirs, preferred_element_type=jnp.float32)
+    own = out_ref.shape[1]
+    groups = begin // own
+    out_ref[:groups] = partial_ref[:begin, :].reshape(groups, own, -1).astype(jnp.bfloat16)
+    out_ref[groups:] = last.reshape(out_ref.shape[0] - groups, own, -1).astype(jnp.bfloat16)
+
+
+def run_down(kernel, name, shape, dtype, *args):
+    in_vmem = pl.BlockSpec(memory_space=pltpu.VMEM)
+    return pl.pallas_call(
+        kernel,
+        out_shape=jax.ShapeDtypeStruct(shape, dtype),
+        in_specs=[in_vmem] * len(args),
+        out_specs=in_vmem,
+        compiler_params=pltpu.CompilerParams(vmem_limit_bytes=8 * 2**20),
+        cost_estimate=pl.CostEstimate(flops=10**8, bytes_accessed=2**21, transcendentals=0),
+        name=name,
+    )(*args)
+
+
 def swap(array, bit):
     pairs = [(i, i ^ bit) for i in range(lax.axis_size("tp"))]
     return lax.ppermute(array, "tp", pairs)
@@ -206,54 +379,40 @@
     )
     mixed, normalizer_new, stab_new, keep, admit, keys, values = run_cell(blocks, heads_here, *held)
     stab_new = stab_new.T
-    projected = jnp.dot(
-        lax.all_gather(mixed, "tp", axis=1, tiled=True),
-        proj_weight,
-        preferred_element_type=jnp.float32,
-    )
-    second = (tokens.astype(jnp.float32) + projected).astype(jnp.bfloat16)
-    second, keep, admit, keys, values = lax.optimization_barrier(
-        (second, keep, admit, keys, values)
-    )
-    keys_f = keys.astype(jnp.float32).reshape(own_rows, heads_here, DK) * DK ** (-0.5)
-    values_f = values.astype(jnp.float32).reshape(own_rows, heads_here, DV)
-    memory_new = (
-        keep[..., None, None] * memory
-        + admit[..., None, None] * values_f[..., :, None] * keys_f[..., None, :]
-    )
-    groups = lax.axis_size("kv")
-    all_rows = lax.all_to_all(
-        jnp.broadcast_to(second, (groups,) + second.shape), "kv", 0, 0, tiled=True
-    ).reshape(groups * own_rows, second.shape[1])
-    scaled = (all_rows.astype(jnp.float32) * ffn_gain).astype(jnp.bfloat16)
-    half = up_weight.shape[1] // 2
-    side = lax.axis_index("tp") % 2
-    mine, theirs = side * half, (1 - side) * half
-    up_mine = lax.dynamic_slice_in_dim(up_weight, mine, half, 1)
-    up_theirs = lax.dynamic_slice_in_dim(up_weight, theirs, half, 1)
-    away = jnp.dot(scaled, up_theirs, preferred_element_type=jnp.float32).astype(jnp.bfloat16)
-    came = swap(away, 1)
-    preact = jnp.dot(scaled, up_mine, preferred_element_type=jnp.float32) + came.astype(jnp.float32)
-    second_f = second.astype(jnp.float32)
-    square_sum = jnp.sum(second_f * second_f, axis=-1, keepdims=True)
+    kv, tp = lax.axis_size("kv"), lax.axis_size("tp")
+    mixed_blocks = [mixed] + [swap(mixed, b) for b in range(1, tp)]
+    memory_new, proj_held = run_update(held[10], keep, admit, keys, values, proj_weight)
+    sent, second, square_sum = run_second(mixed_blocks, proj_held, tokens, kv)
+    all_rows = lax.all_to_all(sent, "kv", 0, 0, tiled=True)
+    away, kept = run_up(all_rows, ffn_gain.reshape(1, -1), up_weight)
+    came = [swap(a, 1) for a in away]
+    came[0], square_sum = lax.optimization_barrier((came[0], square_sum))
+    sent = [(k + c.astype(jnp.float32)).astype(jnp.bfloat16) for k, c in zip(kept, came)]
     square_sum = square_sum + swap(square_sum, 1)
+    sent[-1], square_sum = lax.optimization_barrier((sent[-1], square_sum))
     bit = 2
-    while bit < lax.axis_size("tp"):
-        sent = preact.astype(jnp.bfloat16)
-        preact = sent.astype(jnp.float32) + swap(sent, bit).astype(jnp.float32)
+    while bit < tp:
+        came = [swap(x, bit) for x in sent]
         square_sum = square_sum + swap(square_sum, bit)
+        came[-1], square_sum = lax.optimization_barrier((came[-1], square_sum))
+        preact = [x.astype(jnp.float32) + y.astype(jnp.float32) for x, y in zip(sent, came)]
+        sent = [p.astype(jnp.bfloat16) for p in preact]
         bit *= 2
-    hidden = jnp.square(jax.nn.relu(preact)).astype(jnp.bfloat16)
-    other = swap(hidden, 1)
-    down_mine = lax.dynamic_slice_in_dim(down_weight, mine, half, 0)
-    down_theirs = lax.dynamic_slice_in_dim(down_weight, theirs, half, 0)
-    partial = jnp.dot(hidden, down_mine, preferred_element_type=jnp.float32)
-    partial = partial + jnp.dot(other, down_theirs, preferred_element_type=jnp.float32)
-    sent = partial.astype(jnp.bfloat16).reshape(groups, own_rows, -1)
+    hidden = [jnp.square(jax.nn.relu(p)).astype(jnp.bfloat16) for p in preact]
+    other = [swap(h, 1) for h in hidden]
+    shape = (kv * own_rows, second.shape[1])
+    partial = run_down(
+        down_kernel, "down", shape, jnp.float32, *hidden, *other[:-1], down_weight
+    )
+    sent = run_down(
+        last_kernel, "last", (kv, own_rows, shape[1]), jnp.bfloat16, partial, other[-1], down_weight
+    )
+    scale_two = lax.rsqrt(square_sum / D + EPS)
+    factor = jnp.broadcast_to(scale_two * scale_two, second.shape)
+    sent, factor, second = lax.optimization_barrier((sent, factor, second))
     got = lax.all_to_all(sent, "kv", 0, 0, tiled=True)
     summed = jnp.sum(got.astype(jnp.float32), axis=0)
-    scale_two = lax.rsqrt(square_sum / D + EPS)
-    layer_out = (second_f + summed * (scale_two * scale_two)).astype(jnp.bfloat16)
+    layer_out = (second.astype(jnp.float32) + summed * factor).astype(jnp.bfloat16)
     return (layer_out, memory_new, normalizer_new, stab_new)
 
 

time: 59.8 us -> 57.4 us (0.960)
  blocking collectives: 5.41 us -> 27.8 us
  waiting for transfers between devices: 22.4 us -> 6.93 us
  starting transfers between devices: 16.1 us -> 9.82 us
  Pallas kernels: 6.26 us -> 10.8 us
  other arithmetic: 5.43 us -> 0.95 us
  matrix products: 2.19 us -> 0 us
  local copies, waits for them, and re-layouts: 0.81 us -> 0.09 us
    all_to_all x0 -> x2, blocking collectives: none -> 27.8 us  [the longest x1 15.1 us: per_device(): all_rows = lax.all_to_all(sent, 'kv', 0, 0, tiled=True)]
    all_to_all x2 -> x0, waiting for transfers between devices: 14.4 us -> none  [the longest x1 9.43 us: per_device(): lax.all_to_all(jnp.broadcast_to(second, (groups,) + second.shape), 'kv',...]
    all_to_all x2 -> x0, starting transfers between devices: 9.56 us -> none  [the longest x1 5.98 us: per_device(): lax.all_to_all(jnp.broadcast_to(second, (groups,) + second.shape), 'kv',...]
    all_gather x1 -> x0, blocking collectives: 5.41 us -> none  [per_device(): lax.all_gather(mixed, 'tp', axis=1, tiled=True)]
    pallas_call x0 -> x5, Pallas kernels: none -> 4.51 us  [the longest x1 3.08 us: run_update(): pl.pallas_call(update_kernel, out_shape=[pltpu.HBM(memory.shape, memory.d...]
    add x1, other arithmetic: 4.31 us -> 0.01 us  [per_device(): square_sum = square_sum + swap(square_sum, bit)]
    ppermute x8 -> x14, starting transfers between devices: 6.56 us -> 9.82 us  [swap(): return lax.ppermute(array, 'tp', pairs)]
    dot_general x5 -> x0, matrix products: 2.19 us -> none  [the longest x1 1.01 us: per_device(): jnp.dot(other, down_theirs, preferred_element_type=jnp.float32)]
  transfers between devices with their start and end apart: 10 -> 14, of which waited for: 4 -> 5; matrix products, arithmetic and copies ran while one was open for 10% -> 0% of each run, Pallas kernels for 6% -> 12%
where the time goes in v3:
time: 57.4 us; the launch traced here: 57.1 us
  blocking collectives  27.8 us (48%)
  Pallas kernels  10.8 us (19%)
  starting transfers between devices  9.82 us (17%)
  waiting for transfers between devices  6.93 us (12%)
  other arithmetic  0.95 us (2%)
  between operations  0.82 us (1%)
    all_to_all x1, blocking collectives, per_device(): all_rows = lax.all_to_all(sent, 'kv', 0, 0, tiled=True)  15.1 us
    all_to_all x1, blocking collectives, per_device(): got = lax.all_to_all(sent, 'kv', 0, 0, tiled=True)  12.6 us
    ppermute x14, starting transfers between devices, swap(): return lax.ppermute(array, 'tp', pairs)  9.82 us
    ppermute x14, waiting for transfers between devices, swap(): return lax.ppermute(array, 'tp', pairs)  6.93 us
    pallas_call x1, Pallas kernels, fetch(): pl.pallas_call(functools.partial(fetch_kernel, len(args)), out_shape=[plt...  3.64 us
    pallas_call x1, Pallas kernels, run_update(): pl.pallas_call(update_kernel, out_shape=[pltpu.HBM(memory.shape, memory.d...  3.08 us
    pallas_call x1, Pallas kernels, run_cell(): pl.pallas_call(functools.partial(cell_kernel, heads), out_shape=[jax.Shap...  2.62 us
  transfers between devices with their start and end apart: 14, of which 5 were waited for; matrix products, arithmetic and copies ran while one was open for 0% of the time, Pallas kernels for 12%

profile of v3, /device:TPU:0, one launch (start us, length us, event | category | flops | bytes accessed | tf_op | source)
XLA Modules:
  0.0 57.1 jit_solution(6402830067089965389)
XLA Ops:
  0.6 0.6 collective-permute-start
  1.2 2.6 %collective-permute-start.1 = (bf16[32,512]{1,0:T(8,128)(2,1)}, bf16[32,512]{1,0:T(8,128)(2,1)S(1)}, u32[]{:S(2)}, u32[]{:S(2)}) collective-permute-start(bf16[32,512]{1,0:T(8,128)(2,1)} %refs_5_.1), channel_id=1, source_target_pairs={{0,2},{1,3},{2,0},{3,1},{4,6},{5,7},{6,4},{7,5},{8,10},{9,11},{10,... | collective-permute-start | bytes 98312 | tf_op jit(solution)/shard_map/ppermute | solution.py:341
  3.8 0.0 collective-permute-start.2
  3.8 0.0 copy-start.1
  3.8 3.6 %fetch.1 = (f32[1,2048]{1,0:T(1,128)S(1)}, bf16[2048,256]{1,0:T(8,128)(2,1)S(1)}, bf16[2048,256]{1,0:T(8,128)(2,1)S(1)}, bf16[2048,256]{1,0:T(8,128)(2,1)S(1)}, ...) custom-call(f32[1,2048]{1,0:T(1,128)} %bitcast.11, ...), custom_call_target="tpu_custom_call" | custom-call | flops 1000000000 | bytes 9437184 | tf_op jit(solution)/shard_map/fetch/pallas_call | solution.py:131
  7.5 0.0 collective-permute-done.refs_1_
  7.5 0.0 collective-permute-done.1.refs_2_
  7.5 0.0 collective-permute-done.2.refs_3_
  7.5 0.0 copy-done.1
  7.5 2.6 %cell.1 = (bf16[32,256]{1,0:T(8,128)(2,1)S(1)}, f32[32,2,128]{2,1,0:T(2,128)}, f32[2,32]{1,0:T(2,128)}, f32[32,2]{1,0:T(8,128)S(1)}, f32[32,2]{1,0:T(8,128)S(1)}...) custom-call(bf16[32,512]{1,0:T(8,128)(2,1)S(1)} %copy-done.1, ...), custom_call_target="tpu_custom_call" | custom-call | flops 1000000000 | bytes 9437184 | tf_op jit(solution)/shard_map/cell/pallas_call | solution.py:156
  10.1 0.0 copy-start.2
  10.1 0.0 copy-start.3
  10.1 0.2 collective-permute-start.3
  10.3 1.9 %collective-permute-start.4 = (bf16[32,256]{1,0:T(8,128)(2,1)S(1)}, bf16[32,256]{1,0:T(8,128)(2,1)S(1)}, u32[]{:S(2)}, u32[]{:S(2)}) collective-permute-start(bf16[32,256]{1,0:T(8,128)(2,1)S(1)} %get-tuple-element.53.refs_0_), channel_id=1, source_target_pairs={{0,2},{1,3},{2,0},{3,1},{4,6},{5,7},{6,4},{7,5},{8,10},{9,11},{10,... | collective-permute-start | bytes 49160 | tf_op jit(solution)/shard_map/ppermute | solution.py:341
  12.2 0.0 collective-permute-start.5
  12.2 3.1 %update.1 = (f32[32,2,128,128]{3,2,1,0:T(8,128)}, bf16[1024,512]{1,0:T(8,128)(2,1)S(1)}) custom-call(f32[32,2,128,128]{3,2,1,0:T(8,128)S(1)} %get-tuple-element.51.refs_14_.memory_ref, f32[32,2]{1,0:T(8,128)S(1)} %get-tuple-element.54.keep_ref, f32[32,2]{1,0:T(8,128)S(1)} %get-tuple-element.55.admit_ref, bf16[32,256]{1,0:T(8,128)(2,1)S(1)} %get-tuple-element.56.keys_ref, ...), custom_call_target="tpu_custom_call" | custom-call | flops 1000000000 | bytes 9437184 | tf_op jit(solution)/shard_map/update/pallas_call | solution.py:211
  15.3 0.0 copy-start
  15.3 0.0 collective-permute-done.3.refs_1_
  15.3 0.0 collective-permute-done.4.refs_2_
  15.3 0.2 collective-permute-done.5.refs_3_
  15.5 0.4 second.1
  15.9 15.1 %all_to_all.10.rows_ref = bf16[8,32,512]{2,1,0:T(8,128)(2,1)S(1)} all-to-all(bf16[8,32,512]{2,1,0:T(8,128)(2,1)S(1)} %get-tuple-element.59), channel_id=1, replica_groups=mesh['kv'=8,'tp'=4] {'kv'}, dimensions={0} | all-to-all | bytes 524288 | tf_op jit(solution)/shard_map/all_to_all | solution.py:386
  31.0 0.0 copy-done.2
  31.0 0.0 copy-done.3
  31.0 0.5 up.1
  31.5 0.1 collective-permute-start.6
  31.6 0.5 collective-permute-start.8
  32.1 0.8 %collective-permute-done.6 = bf16[128,512]{1,0:T(8,128)(2,1)S(1)} collective-permute-done((bf16[128,512]{1,0:T(8,128)(2,1)S(1)}, bf16[128,512]{1,0:T(8,128)(2,1)S(1)}, u32[]{:S(2)}, u32[]{:S(2)}) %collective-permute-start.6) | collective-permute-done | bytes 131104 | tf_op jit(solution)/shard_map/ppermute | solution.py:341
  32.9 0.1 collective-permute-start.9
  33.1 1.6 %collective-permute-start.7 = (bf16[128,512]{1,0:T(8,128)(2,1)S(1)}, bf16[128,512]{1,0:T(8,128)(2,1)S(1)}, u32[]{:S(2)}, u32[]{:S(2)}) collective-permute-start(bf16[128,512]{1,0:T(8,128)(2,1)S(1)} %add_convert_fusion.1), channel_id=1, source_target_pairs={{0,2},{1,3},{2,0},{3,1},{4,6},{5,7},{6,4},{7,5},{8,10},{9,11},{10,... | collective-permute-start | bytes 393224 | tf_op jit(solution)/shard_map/ppermute | solution.py:341
  34.7 0.0 collective-permute-done.8
  34.7 0.0 collective-permute-done.9
  34.7 0.9 %collective-permute-start.11 = (f32[32,1]{1,0:T(8,128)S(1)}, f32[32,1]{1,0:T(8,128)S(1)}, u32[]{:S(2)}, u32[]{:S(2)}) collective-permute-start(f32[32,1]{1,0:T(8,128)S(1)} %add.30), channel_id=1, source_target_pairs={{0,2},{1,3},{2,0},{3,1},{4,6},{5,7},{6,4},{7,5},{8,10},{9,11},{10,... | collective-permute-start | bytes 392 | tf_op jit(solution)/shard_map/ppermute | solution.py:341
  35.6 1.2 %collective-permute-start.10 = (bf16[128,512]{1,0:T(8,128)(2,1)S(1)}, bf16[128,512]{1,0:T(8,128)(2,1)S(1)}, u32[]{:S(2)}, u32[]{:S(2)}) collective-permute-start(bf16[128,512]{1,0:T(8,128)(2,1)S(1)} %add_convert_fusion), channel_id=1, source_target_pairs={{0,2},{1,3},{2,0},{3,1},{4,6},{5,7},{6,4},{7,5},{8,10},{9,11},{10,... | collective-permute-start | bytes 393224 | tf_op jit(solution)/shard_map/ppermute | solution.py:341
  36.8 3.0 %collective-permute-done.11 = f32[32,1]{1,0:T(8,128)S(1)} collective-permute-done((f32[32,1]{1,0:T(8,128)S(1)}, f32[32,1]{1,0:T(8,128)S(1)}, u32[]{:S(2)}, u32[]{:S(2)}) %collective-permute-start.11) | collective-permute-done | bytes 160 | tf_op jit(solution)/shard_map/ppermute | solution.py:341
  39.9 0.0 collective-permute-done.7
  39.9 0.1 multiply_convert_fusion.1.refs_0_
  39.9 0.1 collective-permute-start.12
  40.0 2.1 %collective-permute-done.10 = bf16[128,512]{1,0:T(8,128)(2,1)S(1)} collective-permute-done((bf16[128,512]{1,0:T(8,128)(2,1)S(1)}, bf16[128,512]{1,0:T(8,128)(2,1)S(1)}, u32[]{:S(2)}, u32[]{:S(2)}) %collective-permute-start.10) | collective-permute-done | bytes 131104 | tf_op jit(solution)/shard_map/ppermute | solution.py:341
  42.1 0.1 multiply_convert_fusion.refs_1_
  42.1 0.1 collective-permute-start.13
  42.2 0.1 multiply_reduce_fusion
  42.3 0.0 collective-permute-done.12.refs_2_
  42.3 0.0 copy-done
  42.4 0.4 down.1.partial_ref
  42.7 0.8 %collective-permute-done.13.other_ref = bf16[128,512]{1,0:T(8,128)(2,1)S(1)} collective-permute-done((bf16[128,512]{1,0:T(8,128)(2,1)S(1)}, bf16[128,512]{1,0:T(8,128)(2,1)S(1)}, u32[]{:S(2)}, u32[]{:S(2)}) %collective-permute-start.13) | collective-permute-done | bytes 131104 | tf_op jit(solution)/shard_map/ppermute | solution.py:341
  43.5 0.2 last.1
  43.8 0.1 broadcast_in_dim.8
  43.9 12.6 %all_to_all.11 = bf16[8,32,512]{2,1,0:T(8,128)(2,1)S(1)} all-to-all(bf16[8,32,512]{2,1,0:T(8,128)(2,1)S(1)} %last.1), channel_id=1, replica_groups=mesh['kv'=8,'tp'=4] {'kv'}, dimensions={0} | all-to-all | bytes 524288 | tf_op jit(solution)/shard_map/all_to_all | solution.py:413
  56.5 0.6 %add_convert_fusion.2 = bf16[32,512]{1,0:T(8,128)(2,1)} fusion(f32[32,512]{1,0:T(8,128)S(1)} %convert_reduce_fusion, f32[32,512]{1,0:T(8,128)S(1)} %broadcast_in_dim.8, bf16[32,512]{1,0:T(8,128)(2,1)S(1)} %get-tuple-element.72), kind=kLoop, calls=%fused_computation.5 | loop fusion | flops 65536 | bytes 196608 | tf_op jit(solution)/shard_map/convert_element_type | solution.py:415
  (5 shorter events, 0.1 us)
Async XLA Ops:
  0.6 6.8 %collective-permute-start = (bf16[32,512]{1,0:T(8,128)(2,1)}, bf16[32,512]{1,0:T(8,128)(2,1)S(1)}, u32[]{:S(2)}, u32[]{:S(2)}) collective-permute-start(bf16[32,512]{1,0:T(8,128)(2,1)} %refs_5_.1), channel_id=1, source_target_pairs={{0,1},{1,0},{2,3},{3,2},{4,5},{5,4},{6,7},{7,6},{8,9},{9,8},{10,11... | collective-permute-start | bytes 98312 | tf_op jit(solution)/shard_map/ppermute | solution.py:341
  1.2 6.3 %collective-permute-start.1 = (bf16[32,512]{1,0:T(8,128)(2,1)}, bf16[32,512]{1,0:T(8,128)(2,1)S(1)}, u32[]{:S(2)}, u32[]{:S(2)}) collective-permute-start(bf16[32,512]{1,0:T(8,128)(2,1)} %refs_5_.1), channel_id=1, source_target_pairs={{0,2},{1,3},{2,0},{3,1},{4,6},{5,7},{6,4},{7,5},{8,10},{9,11},{10,... | collective-permute-start | bytes 98312 | tf_op jit(solution)/shard_map/ppermute | solution.py:341
  3.8 3.7 %collective-permute-start.2 = (bf16[32,512]{1,0:T(8,128)(2,1)}, bf16[32,512]{1,0:T(8,128)(2,1)S(1)}, u32[]{:S(2)}, u32[]{:S(2)}) collective-permute-start(bf16[32,512]{1,0:T(8,128)(2,1)} %refs_5_.1), channel_id=1, source_target_pairs={{0,3},{1,2},{2,1},{3,0},{4,7},{5,6},{6,5},{7,4},{8,11},{9,10},{10,... | collective-permute-start | bytes 98312 | tf_op jit(solution)/shard_map/ppermute | solution.py:341
  3.8 3.7 %copy-start.1 = (bf16[32,512]{1,0:T(8,128)(2,1)S(1)}, bf16[32,512]{1,0:T(8,128)(2,1)}, u32[]{:S(2)}) copy-start(bf16[32,512]{1,0:T(8,128)(2,1)} %refs_5_.1) | copy-start | bytes 98308
  10.1 20.9 %copy-start.2 = (bf16[512,1024]{1,0:T(8,128)(2,1)S(1)}, bf16[512,1024]{1,0:T(8,128)(2,1)}, u32[]{:S(2)}) copy-start(bf16[512,1024]{1,0:T(8,128)(2,1)} %up_ref.1) | copy-start | bytes 3145732
  10.1 20.9 %copy-start.3 = (f32[512]{0:T(512)S(1)}, f32[512]{0:T(512)}, u32[]{:S(2)}) copy-start(f32[512]{0:T(512)} %param.31) | copy-start | bytes 6148
  10.1 5.2 %collective-permute-start.3 = (bf16[32,256]{1,0:T(8,128)(2,1)S(1)}, bf16[32,256]{1,0:T(8,128)(2,1)S(1)}, u32[]{:S(2)}, u32[]{:S(2)}) collective-permute-start(bf16[32,256]{1,0:T(8,128)(2,1)S(1)} %get-tuple-element.53.refs_0_), channel_id=1, source_target_pairs={{0,1},{1,0},{2,3},{3,2},{4,5},{5,4},{6,7},{7,6},{8,9},{9,8},{10,11... | collective-permute-start | bytes 49160 | tf_op jit(solution)/shard_map/ppermute | solution.py:341
  10.3 5.1 %collective-permute-start.4 = (bf16[32,256]{1,0:T(8,128)(2,1)S(1)}, bf16[32,256]{1,0:T(8,128)(2,1)S(1)}, u32[]{:S(2)}, u32[]{:S(2)}) collective-permute-start(bf16[32,256]{1,0:T(8,128)(2,1)S(1)} %get-tuple-element.53.refs_0_), channel_id=1, source_target_pairs={{0,2},{1,3},{2,0},{3,1},{4,6},{5,7},{6,4},{7,5},{8,10},{9,11},{10,... | collective-permute-start | bytes 49160 | tf_op jit(solution)/shard_map/ppermute | solution.py:341
  12.2 3.3 %collective-permute-start.5 = (bf16[32,256]{1,0:T(8,128)(2,1)S(1)}, bf16[32,256]{1,0:T(8,128)(2,1)S(1)}, u32[]{:S(2)}, u32[]{:S(2)}) collective-permute-start(bf16[32,256]{1,0:T(8,128)(2,1)S(1)} %get-tuple-element.53.refs_0_), channel_id=1, source_target_pairs={{0,3},{1,2},{2,1},{3,0},{4,7},{5,6},{6,5},{7,4},{8,11},{9,10},{10,... | collective-permute-start | bytes 49160 | tf_op jit(solution)/shard_map/ppermute | solution.py:341
  15.3 27.0 %copy-start = (bf16[1024,512]{1,0:T(8,128)(2,1)S(1)}, bf16[1024,512]{1,0:T(8,128)(2,1)}, u32[]{:S(2)}) copy-start(bf16[1024,512]{1,0:T(8,128)(2,1)} %down_ref.1) | copy-start | bytes 3145732
  31.5 1.4 %collective-permute-start.6 = (bf16[128,512]{1,0:T(8,128)(2,1)S(1)}, bf16[128,512]{1,0:T(8,128)(2,1)S(1)}, u32[]{:S(2)}, u32[]{:S(2)}) collective-permute-start(bf16[128,512]{1,0:T(8,128)(2,1)S(1)} %get-tuple-element.61), channel_id=1, source_target_pairs={{0,1},{1,0},{2,3},{3,2},{4,5},{5,4},{6,7},{7,6},{8,9},{9,8},{10,11... | collective-permute-start | bytes 393224 | tf_op jit(solution)/shard_map/ppermute | solution.py:341
  31.6 3.1 %collective-permute-start.8 = (bf16[128,512]{1,0:T(8,128)(2,1)S(1)}, bf16[128,512]{1,0:T(8,128)(2,1)S(1)}, u32[]{:S(2)}, u32[]{:S(2)}) collective-permute-start(bf16[128,512]{1,0:T(8,128)(2,1)S(1)} %get-tuple-element.65), channel_id=1, source_target_pairs={{0,1},{1,0},{2,3},{3,2},{4,5},{5,4},{6,7},{7,6},{8,9},{9,8},{10,11... | collective-permute-start | bytes 393224 | tf_op jit(solution)/shard_map/ppermute | solution.py:341
  32.9 1.8 %collective-permute-start.9 = (f32[32,1]{1,0:T(8,128)S(1)}, f32[32,1]{1,0:T(8,128)S(1)}, u32[]{:S(2)}, u32[]{:S(2)}) collective-permute-start(f32[32,1]{1,0:T(8,128)S(1)} %get-tuple-element.66), channel_id=1, source_target_pairs={{0,1},{1,0},{2,3},{3,2},{4,5},{5,4},{6,7},{7,6},{8,9},{9,8},{10,11... | collective-permute-start | bytes 392 | tf_op jit(solution)/shard_map/ppermute | solution.py:341
  33.1 6.8 %collective-permute-start.7 = (bf16[128,512]{1,0:T(8,128)(2,1)S(1)}, bf16[128,512]{1,0:T(8,128)(2,1)S(1)}, u32[]{:S(2)}, u32[]{:S(2)}) collective-permute-start(bf16[128,512]{1,0:T(8,128)(2,1)S(1)} %add_convert_fusion.1), channel_id=1, source_target_pairs={{0,2},{1,3},{2,0},{3,1},{4,6},{5,7},{6,4},{7,5},{8,10},{9,11},{10,... | collective-permute-start | bytes 393224 | tf_op jit(solution)/shard_map/ppermute | solution.py:341
  34.7 5.1 %collective-permute-start.11 = (f32[32,1]{1,0:T(8,128)S(1)}, f32[32,1]{1,0:T(8,128)S(1)}, u32[]{:S(2)}, u32[]{:S(2)}) collective-permute-start(f32[32,1]{1,0:T(8,128)S(1)} %add.30), channel_id=1, source_target_pairs={{0,2},{1,3},{2,0},{3,1},{4,6},{5,7},{6,4},{7,5},{8,10},{9,11},{10,... | collective-permute-start | bytes 392 | tf_op jit(solution)/shard_map/ppermute | solution.py:341
  35.6 6.4 %collective-permute-start.10 = (bf16[128,512]{1,0:T(8,128)(2,1)S(1)}, bf16[128,512]{1,0:T(8,128)(2,1)S(1)}, u32[]{:S(2)}, u32[]{:S(2)}) collective-permute-start(bf16[128,512]{1,0:T(8,128)(2,1)S(1)} %add_convert_fusion), channel_id=1, source_target_pairs={{0,2},{1,3},{2,0},{3,1},{4,6},{5,7},{6,4},{7,5},{8,10},{9,11},{10,... | collective-permute-start | bytes 393224 | tf_op jit(solution)/shard_map/ppermute | solution.py:341
  39.9 2.4 %collective-permute-start.12 = (bf16[128,512]{1,0:T(8,128)(2,1)S(1)}, bf16[128,512]{1,0:T(8,128)(2,1)S(1)}, u32[]{:S(2)}, u32[]{:S(2)}) collective-permute-start(bf16[128,512]{1,0:T(8,128)(2,1)S(1)} %multiply_convert_fusion.1.refs_0_), channel_id=1, source_target_pairs={{0,1},{1,0},{2,3},{3,2},{4,5},{5,4},{6,7},{7,6},{8,9},{9,8},{10,11... | collective-permute-start | bytes 393224 | tf_op jit(solution)/shard_map/ppermute | solution.py:341
  42.1 1.4 %collective-permute-start.13 = (bf16[128,512]{1,0:T(8,128)(2,1)S(1)}, bf16[128,512]{1,0:T(8,128)(2,1)S(1)}, u32[]{:S(2)}, u32[]{:S(2)}) collective-permute-start(bf16[128,512]{1,0:T(8,128)(2,1)S(1)} %multiply_convert_fusion.refs_1_), channel_id=1, source_target_pairs={{0,1},{1,0},{2,3},{3,2},{4,5},{5,4},{6,7},{7,6},{8,9},{9,8},{10,11... | collective-permute-start | bytes 393224 | tf_op jit(solution)/shard_map/ppermute | solution.py:341
